TPU v7x, 512 devices: a whole 4x8x8 slice. The times are simulated.
512 devices in a mesh: sp: 64 (over z, y), tp: 8 (over x, core).
Axes of the slice: x: 4, y: 8, z: 8, core: 2. Of those that a mesh axis runs over, the one named last changes fastest.
Arguments:
- tokens: bfloat16 [65536, 2048], P(('sp', 'tp')), may hold values from -6 to 6
- norm_gain: float32 [2048], replicated, may hold values from 0.1 to 1.9
- w_query: bfloat16 [2048, 2048], P('sp', 'tp'), may hold values from -0.125 to 0.125
- w_key: bfloat16 [2048, 2048], P('sp', 'tp'), may hold values from -0.125 to 0.125
- w_value: bfloat16 [2048, 4096], P('sp', 'tp'), may hold values from -0.125 to 0.125
- w_rank_down: bfloat16 [2048, 16], replicated, may hold values from -0.125 to 0.125
- w_rank_up: bfloat16 [16, 2048], P(None, 'tp'), may hold values from -1.5 to 1.5
- gate_bias: float32 [2048], P('tp')
- decay_shift: float32 [65536], P('sp'), may hold values from -1 to 0
- out_gain: float32 [512], replicated, may hold values from 0.1 to 1.9
- w_out: bfloat16 [4096, 2048], P('tp', 'sp'), may hold values from -0.09375 to 0.09375
Outputs:
- mixed: bfloat16 [65536, 2048], P(('sp', 'tp'))
All inputs are finite; a program needn't handle non-finite values.
Results may differ from a plain program's by a relative error of at most 0.015.
Values may be sent and summed in bfloat16 or wider, within the bound.
A program may use at most 128 MiB of HBM per device.

v0:
```python
import jax
import jax.numpy as jnp
from jax import lax
from jax.sharding import Mesh
from jax.sharding import PartitionSpec as P

DK = 256
DV = 512
TAU = 16
BLOCK = 64
SP = ("sp_0", "sp_1")
SP_TP = ("sp_0", "sp_1", "tp")


EPS = 1e-06


def sent_together(arrays, axis, dim, along):
    both = jnp.concatenate(arrays, axis=along)
    out, at, finished = (lax.all_gather(both, axis, axis=dim, tiled=True), 0, [])
    for a in arrays:
        finished.append(lax.slice_in_dim(out, at, at + a.shape[along], axis=along))
        at += a.shape[along]
    return tuple(finished)


def filled_with(value, identity):
    return jax.tree.map(
        lambda a, e: jnp.broadcast_to(jnp.asarray(e, a.dtype), a.shape), value, identity
    )


def entering(value, axes, combine, identity):
    before = start = filled_with(value, identity)
    total = value
    for axis in reversed(axes):
        size, mine = (lax.axis_size(axis), lax.axis_index(axis))
        pieces = jax.tree.map(lambda part: lax.all_gather(part, axis), total)
        inside, total = (start, start)
        for k in range(size):
            passed = k < mine
            total = combine(total, jax.tree.map(lambda part: part[k], pieces))
            inside = jax.tree.map(lambda new, old: jnp.where(passed, new, old), total, inside)
        before = combine(inside, before)
    return before


def cut_along(value, dim, size):
    before, after = (value.shape[:dim], value.shape[dim + 1 :])
    return jnp.moveaxis(value.reshape(*before, size, -1, *after), dim, 0)


def sent_and_summed(value, axis, dim):
    size = lax.axis_size(axis)
    parts = lax.all_to_all(cut_along(value, dim, size), axis, 0, 0, tiled=True)
    return jnp.sum(parts.astype(jnp.float32), axis=0)


def rms_rows(values, gain):
    wide = values.astype(jnp.float32)
    return wide * lax.rsqrt(jnp.mean(wide * wide, axis=-1, keepdims=True) + EPS) * gain


def local_pass(query, key, value, log_decay, state):
    rows, heads, width = query.shape
    blocks = rows // BLOCK

    def split(tensor):
        return tensor.reshape((blocks, BLOCK) + tensor.shape[1:])

    causal = jnp.tril(jnp.ones((BLOCK, BLOCK), dtype=bool))

    def local_step(carry, inputs):
        q_blk, k_blk, v_blk, g_blk = inputs
        cumul = jnp.cumsum(g_blk, axis=0)
        centre = cumul - cumul[BLOCK // 2]
        q_scaled = (q_blk * jnp.exp(centre)).astype(jnp.bfloat16)
        k_scaled = (k_blk * jnp.exp(-centre)).astype(jnp.bfloat16)
        scores = jnp.einsum("ihd,jhd->hij", q_scaled, k_scaled, preferred_element_type=jnp.float32)
        scores = jnp.where(causal[None], scores, 0.0).astype(jnp.bfloat16)
        within = jnp.einsum("hij,jhe->ihe", scores, v_blk, preferred_element_type=jnp.float32)
        final = cumul[-1]
        decayed = (k_blk * jnp.exp(final - cumul)).astype(jnp.bfloat16)
        nxt = jnp.exp(final)[:, :, None] * carry + jnp.einsum(
            "jhd,jhe->hde", decayed, v_blk, preferred_element_type=jnp.float32
        )
        return (nxt, (within, q_blk * jnp.exp(cumul), final, carry))

    carry, (within, reach, finals, starts) = lax.scan(
        local_step, state, (split(query), split(key), split(value), split(log_decay))
    )
    return (within, reach, finals, starts, carry)


def state_only(key, value, log_decay, state):
    rows, heads, width = key.shape
    blocks = rows // BLOCK

    def split(tensor):
        return tensor.reshape((blocks, BLOCK) + tensor.shape[1:])

    def state_step(carry, inputs):
        k_blk, v_blk, g_blk = inputs
        cumul = jnp.cumsum(g_blk, axis=0)
        final = cumul[-1]
        decayed = (k_blk * jnp.exp(final - cumul)).astype(jnp.bfloat16)
        carry = jnp.exp(final)[:, :, None] * carry + jnp.einsum(
            "jhd,jhe->hde", decayed, v_blk, preferred_element_type=jnp.float32
        )
        return (carry, final)

    carry, finals = lax.scan(state_step, state, (split(key), split(value), split(log_decay)))
    return (carry, finals)


def read_out(reach, starts):
    blocks, block, heads, width = reach.shape
    result = jnp.einsum(
        "nihd,nhde->nihe",
        reach.astype(jnp.bfloat16),
        starts.astype(jnp.bfloat16),
        preferred_element_type=jnp.float32,
    )
    return result.reshape(blocks * block, heads, -1)


def combine(earlier, later):
    return (earlier[0] * later[0], later[0][:, :, None] * earlier[1] + later[1])


def on_device(
    tokens,
    norm_gain,
    w_query,
    w_key,
    w_value,
    w_rank_down,
    w_rank_up,
    gate_bias,
    decay_shift,
    out_gain,
    w_out,
):
    normed = rms_rows(tokens, norm_gain).astype(jnp.bfloat16)
    query_w, key_w, value_w = sent_together((w_query, w_key, w_value), SP, 0, 1)
    keys_here = query_w.shape[1]
    vals_here = value_w.shape[1]
    heads_here = keys_here // DK
    w_joined = jnp.concatenate([query_w, key_w, value_w, w_rank_down], axis=1)
    joined = jnp.dot(
        lax.all_gather(normed, "tp", axis=0, tiled=True),
        w_joined,
        preferred_element_type=jnp.float32,
    ).astype(jnp.bfloat16)
    span = joined.shape[0]
    q_heads = joined[:, :keys_here].astype(jnp.float32).reshape(span, heads_here, DK) * DK ** (-0.5)
    k_heads = joined[:, keys_here : 2 * keys_here].astype(jnp.float32).reshape(span, heads_here, DK)
    v_heads = joined[:, 2 * keys_here : 2 * keys_here + vals_here].reshape(span, heads_here, DV)
    rank = joined[:, 2 * keys_here + vals_here :]
    pre = jnp.dot(rank, w_rank_up, preferred_element_type=jnp.float32) + gate_bias
    log_decay = (jax.nn.log_sigmoid(pre) / TAU + decay_shift[:, None]).reshape(span, heads_here, DK)
    empty = jnp.zeros((heads_here, DK, DV), jnp.float32)
    identity = (jnp.ones((heads_here, DK), jnp.float32), empty)
    local_end, finals = state_only(k_heads, v_heads, log_decay, empty)
    carried = entering((jnp.exp(jnp.sum(finals, axis=0)), local_end), SP, combine, identity)[1]
    within, reach, _, starts, _ = local_pass(q_heads, k_heads, v_heads, log_decay, carried)
    attended = within.reshape(span, heads_here, DV) + read_out(reach, starts)
    shaped = rms_rows(attended, out_gain).astype(jnp.bfloat16).reshape(span, heads_here * DV)
    out_whole = lax.all_gather(w_out, SP, axis=1, tiled=True)
    return sent_and_summed(
        jnp.dot(shaped, out_whole, preferred_element_type=jnp.float32).astype(jnp.bfloat16), "tp", 0
    ).astype(jnp.bfloat16)


def solution(mesh):
    finer = Mesh(mesh.devices.reshape(8, 8, mesh.shape["tp"]), ("sp_0", "sp_1", "tp"))
    in_specs = (
        P(SP_TP, None),
        P(),
        P(SP, "tp"),
        P(SP, "tp"),
        P(SP, "tp"),
        P(),
        P(None, "tp"),
        P("tp"),
        P(SP),
        P(),
        P("tp", SP),
    )
    out_specs = P(SP_TP, None)
    return jax.shard_map(
        on_device, mesh=finer, in_specs=in_specs, out_specs=out_specs, check_vma=False
    )
```

profile of v0, /device:TPU:1, one launch (start us, length us, event | category | flops | bytes accessed | tf_op | source)
XLA Modules:
  0.0 498.0 jit_solution(9612616746641343713)
XLA Ops:
  6.5 1.2 fusion.59
  7.8 2.0 fusion.61
  9.9 1.4 pad_maximum_fusion
  12.5 40.7 %all-gather.9.cloned.1.call-done = bf16[1024,2048]{1,0:T(8,128)(2,1)} async-done(((bf16[128,2048]{1,0:T(8,128)(2,1)}), bf16[1024,2048]{1,0:T(8,128)(2,1)}) %all-gather.9.cloned.1.call-update) | async-done | bytes 4194320 | tf_op jit(solution)/shard_map/all_gather | solution.py:151
  53.2 85.4 %all-gather.11.cloned.1.call-done = bf16[2048,1024]{1,0:T(8,128)(2,1)} async-done(((bf16[32,1024]{1,0:T(8,128)(2,1)}), bf16[2048,1024]{1,0:T(8,128)(2,1)}) %all-gather.11.cloned.1.call-update) | async-done | bytes 4194320 | tf_op jit(solution)/shard_map/all_gather | solution.py:20
  138.6 8.1 %fusion.51 = bf16[1024,1040]{0,1:T(8,128)(2,1)S(1)} fusion(bf16[1024,2048]{1,0:T(8,128)(2,1)} %all-gather.9.cloned.1.call-done, bf16[2048,16]{1,0:T(8,128)(2,1)S(1)} %copy.37, bf16[2048,1024]{1,0:T(8,128)(2,1)} %all-gather.11.cloned.1.call-done), kind=kOutput, calls=%fused_computation.62 | convolution fusion | flops 4371660800 | bytes 10584064 | tf_op jit(solution)/shard_map/dot_general | solution.py:150
  146.7 1.2 slice_convert_fusion
  148.0 1.9 fusion.64
  149.8 2.5 copy.39
  152.4 3.4 copy.42
  155.8 1.6 copy.40
  157.3 2.1 copy.43
  159.4 1.3 copy.41
  160.7 48.5 %while.31 = (s32[]{:T(128)}, f32[1,256,512]{2,1,0:T(8,128)S(1)}, f32[16,1,256]{2,1,0:T(1,128)S(1)}, f32[16,64,1,256]{3,2,1,0:T(1,128)}, f32[16,64,1,256]{3,2,1,0...) while((s32[]{:T(128)}, f32[1,256,512]{2,1,0:T(8,128)S(1)}, ...), condition=%wide.region_3.4_spmd.clone, body=%wide.region_1.3_spmd.clone.sunk | while | flops 18251780 | bytes 1450087 | solution.py:112
  210.2 11.0 %all-gather.2 = f32[8,1,256]{2,1,0:T(1,128)S(1)} all-gather(f32[1,1,256]{2,1,0:T(1,128)S(1)} %bitcast.299), channel_id=2, replica_groups=mesh['sp_0'=8,'sp_1'=8,'tp'=8] {'sp_1'}, dimensions={0}, use_global_device_ids=true | all-gather | bytes 9216 | tf_op jit(solution)/shard_map/all_gather | solution.py:38
  221.2 46.4 %all-gather.17.cloned.1.call-done = f32[8,256,512]{2,1,0:T(8,128)} async-done(((f32[1,256,512]{2,1,0:T(8,128)}), f32[8,256,512]{2,1,0:T(8,128)}) %all-gather.17.cloned.1.call-update) | async-done | bytes 4194320 | tf_op jit(solution)/shard_map/all_gather | solution.py:38
  267.6 3.3 bitcast_add_fusion.1
  271.7 13.7 %all_gather.30 = f32[8,1,256]{2,1,0:T(1,128)S(1)} all-gather(f32[1,1,256]{2,1,0:T(1,128)S(1)} %get-tuple-element.230), channel_id=1, replica_groups=mesh['sp_0'=8,'sp_1'=8,'tp'=8] {'sp_0'}, dimensions={0}, use_global_device_ids=true | all-gather | bytes 9216 | tf_op jit(solution)/shard_map/all_gather | solution.py:38
  285.7 42.6 %all-gather.13.cloned.1.call-done = f32[8,1,256,512]{3,2,1,0:T(8,128)} async-done(((f32[1,1,256,512]{3,2,1,0:T(8,128)}), f32[8,1,256,512]{3,2,1,0:T(8,128)}) %all-gather.13.cloned.1.call-update) | async-done | bytes 4194320 | tf_op jit(solution)/shard_map/all_gather | solution.py:38
  328.3 4.3 fusion.68
  332.6 93.2 %while.30 = (s32[]{:T(128)}, f32[1,256,512]{2,1,0:T(8,128)S(1)}, f32[16,64,1,512]{3,1,2,0:T(8,128)}, bf16[16,64,1,256]{3,1,0,2:T(8,128)(2,1)S(1)}, bf16[16,1,256...) while((s32[]{:T(128)}, f32[1,256,512]{2,1,0:T(8,128)S(1)}, ...), condition=%wide.region_7.8_spmd.clone, body=%wide.region_5.7_spmd.clone.sunk | while | flops 24555520 | bytes 3223153 | solution.py:89
  334.8 1.8 fusion.117
  337.3 1.1 fusion.116
  340.6 1.8 fusion.117
  343.1 1.1 fusion.116
  346.4 1.8 fusion.117
  348.9 1.1 fusion.116
  352.2 1.8 fusion.117
  358.0 1.8 fusion.117
  363.9 1.8 fusion.117
  369.7 1.8 fusion.117
  375.5 1.8 fusion.117
  378.1 1.1 fusion.116
  381.4 1.8 fusion.117
  387.2 1.8 fusion.117
  389.7 1.1 fusion.116
  393.0 1.8 fusion.117
  398.9 1.8 fusion.117
  401.4 1.1 fusion.116
  404.7 1.8 fusion.117
  407.2 1.1 fusion.116
  410.5 1.8 fusion.117
  416.3 1.8 fusion.117
  422.2 1.8 fusion.117
  425.8 3.8 multiply_reduce_fusion
  430.0 4.0 convolution_convert_fusion
  434.0 53.6 %all_to_all.5 = bf16[8,128,2048]{2,1,0:T(8,128)(2,1)} all-to-all(bf16[8,128,2048]{2,1,0:T(8,128)(2,1)S(1)} %bitcast.263), channel_id=1, replica_groups=mesh['sp_0'=8,'sp_1'=8,'tp'=8] {'tp'}, dimensions={0} | all-to-all | bytes 8388608 | tf_op jit(solution)/shard_map/all_to_all | solution.py:55
  487.7 3.8 reduce_sum.42
  (249 shorter events, 107.3 us)
Async XLA Ops:
  6.5 141.4 %copy-start = (bf16[16,256]{1,0:T(8,128)(2,1)S(1)}, bf16[16,256]{1,0:T(8,128)(2,1)}, u32[]{:S(2)}) copy-start(bf16[16,256]{1,0:T(8,128)(2,1)} %param.21) | copy-start | bytes 24580
  6.5 46.7 %all-gather.9.cloned.1.call-start = ((), (), s32[]{:S(2)}) async-start(), calls=%async_computation.1 | async-start | bytes 4718592 | tf_op jit(solution)/shard_map/all_gather | solution.py:151
  9.8 128.8 %all-gather.11.cloned.1.call-start = ((), (), s32[]{:S(2)}) async-start(), calls=%async_computation.2 | async-start | bytes 4259840 | tf_op jit(solution)/shard_map/all_gather | solution.py:20
  11.3 256.3 %all-gather.17.cloned.1.call-start = ((), (), s32[]{:S(2)}) async-start(), calls=%async_computation.5 | async-start | bytes 4718592 | tf_op jit(solution)/shard_map/all_gather | solution.py:38
  12.5 135.5 %copy-start.6 = (f32[1024]{0:T(1024)S(1)}, f32[1024]{0:T(1024)}, u32[]{:S(2)}) copy-start(f32[1024]{0:T(1024)} %param.23) | copy-start | bytes 12292
  12.5 135.4 %copy-start.7 = (f32[256]{0:T(256)S(1)}, f32[256]{0:T(256)}, u32[]{:S(2)}) copy-start(f32[256]{0:T(256)} %param.22) | copy-start | bytes 3076
  146.7 5.6 %copy-start.2 = (bf16[1024,1040]{0,1:T(8,128)(2,1)}, bf16[1024,1040]{0,1:T(8,128)(2,1)S(1)}, u32[]{:S(2)}) copy-start(bf16[1024,1040]{0,1:T(8,128)(2,1)S(1)} %fusion.51) | copy-start | bytes 6389764
  152.4 7.1 %slice-start = ((bf16[1024,1040]{0,1:T(8,128)(2,1)}), bf16[1024,512]{0,1:T(8,128)(2,1)S(1)}, s32[]{:S(2)}) async-start(bf16[1024,1040]{0,1:T(8,128)(2,1)} %copy-done.2), calls=%async_computation.6 | async-start | bytes 2097152 | tf_op jit(solution)/shard_map/slice | solution.py:158
  209.2 0.8 copy-start.1
  209.2 62.3 %copy-start.3 = (bf16[1024,1040]{0,1:T(8,128)(2,1)S(1)}, bf16[1024,1040]{0,1:T(8,128)(2,1)}, u32[]{:S(2)}) copy-start(bf16[1024,1040]{0,1:T(8,128)(2,1)} %copy-done.2) | copy-start | bytes 6389764
  210.0 118.2 %all-gather.13.cloned.1.call-start = ((), (), s32[]{:S(2)}) async-start(), calls=%async_computation.3 | async-start | bytes 4718592 | tf_op jit(solution)/shard_map/all_gather | solution.py:38
  270.9 159.1 %all-gather.15.cloned.1.call-start = ((), (), s32[]{:S(2)}) async-start(), calls=%async_computation.4 | async-start | bytes 2129920 | tf_op jit(solution)/shard_map/all_gather | solution.py:169
  328.3 4.3 copy-start.4
  425.8 3.9 copy-start.5
Sparse Core Ops, SparseCore 0:
  10.0 43.2 all-gather.8
  56.3 82.2 all-gather.10
  210.2 57.3 all-gather.16
  271.0 57.2 all-gather.12
  331.2 77.5 all-gather.14
where the time goes:
time: 504 us; the launch traced here: 498 us
  waiting for transfers between devices  216 us (43%)
  matrix products  82.2 us (16%)
  other arithmetic  81 us (16%)
  blocking collectives  78.3 us (16%)
  local copies, waits for them, and re-layouts  25.8 us (5%)
  between operations  13.4 us (3%)
    all_gather x2, waiting for transfers between devices, entering(): pieces = jax.tree.map(lambda part: lax.all_gather(part, axis), total)  89 us
    all_gather x1, waiting for transfers between devices, sent_together(): lax.all_gather(both, axis, axis=dim, tiled=True)  85.4 us
    all_to_all x1, blocking collectives, sent_and_summed(): parts = lax.all_to_all(cut_along(value, dim, size), axis, 0, 0, tiled=True)  53.6 us
    all_gather x1, waiting for transfers between devices, on_device(): lax.all_gather(normed, 'tp', axis=0, tiled=True)  40.7 us
    dot_general x16, matrix products, local_step(): jnp.einsum('hij,jhe->ihe', scores, v_blk, preferred_element_type=jnp.floa...  28.5 us
    all_gather x2, blocking collectives, entering(): pieces = jax.tree.map(lambda part: lax.all_gather(part, axis), total)  24.7 us
    dot_general x16, matrix products, local_step(): jnp.einsum('jhd,jhe->hde', decayed, v_blk, preferred_element_type=jnp.flo...  18.3 us
    dot_general x16, matrix products, state_step(): jnp.einsum('jhd,jhe->hde', decayed, v_blk, preferred_element_type=jnp.flo...  17.7 us
  transfers between devices with their start and end apart: 5, of which 4 were waited for; matrix products, arithmetic and copies ran while one was open for 21% of the time, Pallas kernels for 0%

commit v1 on v0

v1 whole, which is shorter than its diff:
```python
import jax
import jax.numpy as jnp
from jax import lax
from jax.experimental import pallas as pl
from jax.experimental.pallas import tpu as pltpu
from jax.sharding import Mesh
from jax.sharding import PartitionSpec as P

DK = 256
DV = 512
TAU = 16
BLOCK = 64
QUAD = 256
SP = ("sp_0", "sp_1")
SP_TP = ("sp_0", "sp_1", "tp")
EPS = 1e-06
VMEM = pl.BlockSpec(memory_space=pltpu.VMEM)


def sent_together(arrays, axis, dim, along):
    both = jnp.concatenate(arrays, axis=along)
    out, at, finished = (lax.all_gather(both, axis, axis=dim, tiled=True), 0, [])
    for a in arrays:
        finished.append(lax.slice_in_dim(out, at, at + a.shape[along], axis=along))
        at += a.shape[along]
    return tuple(finished)


def filled_with(value, identity):
    return jax.tree.map(
        lambda a, e: jnp.broadcast_to(jnp.asarray(e, a.dtype), a.shape), value, identity
    )


def entering(value, axes, combine, identity):
    before = start = filled_with(value, identity)
    total = value
    for axis in reversed(axes):
        size, mine = (lax.axis_size(axis), lax.axis_index(axis))
        pieces = jax.tree.map(lambda part: lax.all_gather(part, axis), total)
        inside, total = (start, start)
        for k in range(size):
            passed = k < mine
            total = combine(total, jax.tree.map(lambda part: part[k], pieces))
            inside = jax.tree.map(lambda new, old: jnp.where(passed, new, old), total, inside)
        before = combine(inside, before)
    return before


def cut_along(value, dim, size):
    before, after = (value.shape[:dim], value.shape[dim + 1 :])
    return jnp.moveaxis(value.reshape(*before, size, -1, *after), dim, 0)


def sent_and_summed(value, axis, dim):
    size = lax.axis_size(axis)
    parts = lax.all_to_all(cut_along(value, dim, size), axis, 0, 0, tiled=True)
    return jnp.sum(parts.astype(jnp.float32), axis=0)


def rms_rows(values, gain):
    wide = values.astype(jnp.float32)
    return wide * lax.rsqrt(jnp.mean(wide * wide, axis=-1, keepdims=True) + EPS) * gain


def combine(earlier, later):
    return (earlier[0] * later[0], later[0][None, :] * earlier[1] + later[1])


def dot(a, b, dims):
    return lax.dot_general(a, b, (dims, ((), ())), preferred_element_type=jnp.float32)


NN, NT, TN = (((1,), (0,)), ((1,), (1,)), ((0,), (0,)))


def block_masks():
    row = lax.broadcasted_iota(jnp.int32, (QUAD, QUAD), 0)
    col = lax.broadcasted_iota(jnp.int32, (QUAD, QUAD), 1)
    return (row // BLOCK == col // BLOCK) & (col <= row)


def local_kernel(x_ref, up_ref, bias_ref, shift_ref, att_ref, far_ref, state_ref, total_ref):
    rows = x_ref.shape[0]
    state_ref[...] = jnp.zeros_like(state_ref)
    total_ref[...] = jnp.zeros_like(total_ref)
    nb = QUAD // BLOCK

    def body(i, carry):
        at = pl.ds(pl.multiple_of(i * QUAD, QUAD), QUAD)
        causal = block_masks()
        lower = jnp.where(causal, 1.0, 0.0).astype(jnp.bfloat16)
        pre = dot(x_ref[at, 1024:1040], up_ref[...], NN) + bias_ref[...]
        logs = jnp.minimum(pre, 0.0) - jnp.log1p(jnp.exp(-jnp.abs(pre)))
        decay = logs * (1.0 / TAU) + shift_ref[at, :]
        hi = decay.astype(jnp.bfloat16)
        rest = decay - hi.astype(jnp.float32)
        mid = rest.astype(jnp.bfloat16)
        low = (rest - mid.astype(jnp.float32)).astype(jnp.bfloat16)
        cumul = dot(lower, hi, NN) + (dot(lower, mid, NN) + dot(lower, low, NN))
        cube = cumul.reshape(nb, BLOCK, DK)
        middle, final = (cube[:, BLOCK // 2 : BLOCK // 2 + 1], cube[:, BLOCK - 1 : BLOCK])
        centre = (cube - middle).reshape(QUAD, DK)
        tail = (final - cube).reshape(QUAD, DK)
        q = x_ref[at, 0:DK].astype(jnp.float32) * DK ** (-0.5)
        k = x_ref[at, DK : 2 * DK].astype(jnp.float32)
        q_scaled = (q * jnp.exp(centre)).astype(jnp.bfloat16)
        k_scaled = (k * jnp.exp(-centre)).astype(jnp.bfloat16)
        reach = q * jnp.exp(cumul)
        decayed = (k * jnp.exp(tail)).astype(jnp.bfloat16)
        v = x_ref[at, 2 * DK : 2 * DK + DV]
        scores = jnp.where(causal, dot(q_scaled, k_scaled, NT), 0.0).astype(jnp.bfloat16)
        within = dot(scores, v, NN)
        for n in range(nb):
            part = slice(n * BLOCK, (n + 1) * BLOCK)
            base = total_ref[...]
            rows_at = pl.ds(pl.multiple_of(i * QUAD + n * BLOCK, BLOCK), BLOCK)
            far_ref[rows_at, :] = (reach[part] * jnp.exp(base)).astype(jnp.bfloat16)
            state = state_ref[...]
            read = dot(reach[part].astype(jnp.bfloat16), state.astype(jnp.bfloat16), NT)
            att_ref[rows_at, :] = within[part] + read
            state_ref[...] = jnp.exp(final[n]) * state + dot(v[part], decayed[part], TN)
            total_ref[...] = base + final[n]
        return carry

    lax.fori_loop(0, rows // QUAD, body, 0)


def finish_kernel(att_ref, far_ref, carried_ref, gain_ref, out_w_ref, part_ref):
    rows = att_ref.shape[0]

    def body(i, carry):
        at = pl.ds(pl.multiple_of(i * QUAD, QUAD), QUAD)
        att = att_ref[at, :] + dot(far_ref[at, :], carried_ref[...], NT)
        shaped = att * lax.rsqrt(jnp.mean(att * att, axis=-1, keepdims=True) + EPS) * gain_ref[...]
        part_ref[at, :] = dot(shaped.astype(jnp.bfloat16), out_w_ref[...], NN).astype(jnp.bfloat16)
        return carry

    lax.fori_loop(0, rows // QUAD, body, 0)


def on_device(
    tokens,
    norm_gain,
    w_query,
    w_key,
    w_value,
    w_rank_down,
    w_rank_up,
    gate_bias,
    decay_shift,
    out_gain,
    w_out,
):
    normed = rms_rows(tokens, norm_gain).astype(jnp.bfloat16)
    query_w, key_w, value_w = sent_together((w_query, w_key, w_value), SP, 0, 1)
    w_joined = jnp.concatenate([query_w, key_w, value_w, w_rank_down], axis=1)
    joined = jnp.dot(
        lax.all_gather(normed, "tp", axis=0, tiled=True),
        w_joined,
        preferred_element_type=jnp.float32,
    ).astype(jnp.bfloat16)
    span = joined.shape[0]
    att, far, local_end, total = pl.pallas_call(
        local_kernel,
        out_shape=(
            jax.ShapeDtypeStruct((span, DV), jnp.float32),
            jax.ShapeDtypeStruct((span, DK), jnp.bfloat16),
            jax.ShapeDtypeStruct((DV, DK), jnp.float32),
            jax.ShapeDtypeStruct((1, DK), jnp.float32),
        ),
        in_specs=[VMEM] * 4,
        out_specs=(VMEM,) * 4,
    )(joined, w_rank_up, gate_bias[None], decay_shift[:, None])
    identity = (jnp.ones((DK,), jnp.float32), jnp.zeros((DV, DK), jnp.float32))
    carried = entering((jnp.exp(total[0]), local_end), SP, combine, identity)[1]
    out_whole = lax.all_gather(w_out, SP, axis=1, tiled=True)
    partial = pl.pallas_call(
        finish_kernel,
        out_shape=jax.ShapeDtypeStruct((span, out_whole.shape[1]), jnp.bfloat16),
        in_specs=[VMEM] * 5,
        out_specs=VMEM,
    )(att, far, carried.astype(jnp.bfloat16), out_gain[None], out_whole)
    return sent_and_summed(partial, "tp", 0).astype(jnp.bfloat16)


def solution(mesh):
    finer = Mesh(mesh.devices.reshape(8, 8, mesh.shape["tp"]), ("sp_0", "sp_1", "tp"))
    in_specs = (
        P(SP_TP, None),
        P(),
        P(SP, "tp"),
        P(SP, "tp"),
        P(SP, "tp"),
        P(),
        P(None, "tp"),
        P("tp"),
        P(SP),
        P(),
        P("tp", SP),
    )
    out_specs = P(SP_TP, None)
    return jax.shard_map(
        on_device, mesh=finer, in_specs=in_specs, out_specs=out_specs, check_vma=False
    )
```

time: 504 us -> 437 us (0.87); the launches traced: 498 us -> 437 us
  waiting for transfers between devices: 216 us -> 294 us
  matrix products: 82.2 us -> 8.09 us
  other arithmetic: 81 us -> 16.7 us
  Pallas kernels: 0 us -> 18.1 us
  local copies, waits for them, and re-layouts: 25.8 us -> 9.99 us
    all_gather x1, waiting for transfers between devices: 0.02 us -> 78 us  [on_device(): out_whole = lax.all_gather(w_out, SP, axis=1, tiled=True)]
    dot_general x51 -> x0, matrix products: 74.1 us -> none  [the longest x16 28.5 us: local_step(): jnp.einsum('hij,jhe->ihe', scores, v_blk, preferred_element_type=jnp.floa...]
    another operation x33 -> x0, other arithmetic: 31.6 us -> none  [the longest x16 15.8 us: local_step(): cumul = jnp.cumsum(g_blk, axis=0)]
    convert_element_type x33 -> x1, other arithmetic: 33 us -> 4.96 us  [on_device(): carried.astype(jnp.bfloat16)]
    pallas_call x0 -> x2, Pallas kernels: none -> 18.1 us  [the longest x1 9.76 us: on_device(): pl.pallas_call(local_kernel, out_shape=(jax.ShapeDtypeStruct((span, DV),...]
    dynamic_update_slice x48 -> x0, local copies, waits for them, and re-layouts: 12.2 us -> none  [the longest x32 12 us: local_pass(): lax.scan(local_step, state, (split(query), split(key), split(value), spli...]
    unnamed x19 -> x2, local copies, waits for them, and re-layouts: 7.42 us -> 1.78 us
  transfers between devices with their start and end apart: 5 -> 5, of which waited for: 4 -> 5; matrix products, arithmetic and copies ran while one was open for 21% -> 3% of each run, Pallas kernels for 0% -> 0%
where the time goes in v1:
time: 437 us
  waiting for transfers between devices  294 us (67%)
  blocking collectives  76 us (17%)
  Pallas kernels  18.1 us (4%)
  other arithmetic  16.7 us (4%)
  between operations  13.2 us (3%)
  local copies, waits for them, and re-layouts  9.99 us (2%)
  matrix products  8.09 us (2%)
    all_gather x2, waiting for transfers between devices, entering(): pieces = jax.tree.map(lambda part: lax.all_gather(part, axis), total)  91.3 us
    all_gather x1, waiting for transfers between devices, sent_together(): lax.all_gather(both, axis, axis=dim, tiled=True)  85.4 us
    all_gather x1, waiting for transfers between devices, on_device(): out_whole = lax.all_gather(w_out, SP, axis=1, tiled=True)  78 us
    all_to_all x1, blocking collectives, sent_and_summed(): parts = lax.all_to_all(cut_along(value, dim, size), axis, 0, 0, tiled=True)  53.9 us
    all_gather x1, waiting for transfers between devices, on_device(): lax.all_gather(normed, 'tp', axis=0, tiled=True)  39 us
    all_gather x2, blocking collectives, entering(): pieces = jax.tree.map(lambda part: lax.all_gather(part, axis), total)  22.1 us
    pallas_call x1, Pallas kernels, on_device(): pl.pallas_call(local_kernel, out_shape=(jax.ShapeDtypeStruct((span, DV),...  9.76 us
  transfers between devices with their start and end apart: 5, of which 5 were waited for; matrix products, arithmetic and copies ran while one was open for 3% of the time, Pallas kernels for 0%

profile of v1, /device:TPU:1, one launch (start us, length us, event | category | flops | bytes accessed | tf_op | source)
XLA Modules:
  0.0 436.6 jit_solution(1749379771710777049)
XLA Ops:
  6.5 0.0 all-gather.9.cloned.1.call-start
  6.5 1.2 fusion.7
  7.8 2.0 fusion.9
  9.8 0.0 all-gather.9.cloned.1.call-update
  9.8 0.0 all-gather.11.cloned.1.call-start
  9.9 1.4 pad_maximum_fusion
  11.3 0.0 all-gather.11.cloned.1.call-update
  11.3 0.0 all-gather.17.cloned.1.call-start
  11.3 1.1 copy.23
  12.5 1.7 copy.25.shift_ref
  14.2 39.0 %all-gather.9.cloned.1.call-done = bf16[1024,2048]{1,0:T(8,128)(2,1)} async-done(((bf16[128,2048]{1,0:T(8,128)(2,1)}), bf16[1024,2048]{1,0:T(8,128)(2,1)}) %all-gather.9.cloned.1.call-update) | async-done | bytes 4194320 | tf_op jit(solution)/shard_map/all_gather | solution.py:159
  53.2 85.4 %all-gather.11.cloned.1.call-done = bf16[2048,1024]{1,0:T(8,128)(2,1)} async-done(((bf16[32,1024]{1,0:T(8,128)(2,1)}), bf16[2048,1024]{1,0:T(8,128)(2,1)}) %all-gather.11.cloned.1.call-update) | async-done | bytes 4194320 | tf_op jit(solution)/shard_map/all_gather | solution.py:22
  138.6 8.1 %fusion.4 = bf16[1024,1040]{0,1:T(8,128)(2,1)S(1)} fusion(bf16[1024,2048]{1,0:T(8,128)(2,1)} %all-gather.9.cloned.1.call-done, bf16[2048,16]{1,0:T(8,128)(2,1)S(1)} %copy.23, bf16[2048,1024]{1,0:T(8,128)(2,1)} %all-gather.11.cloned.1.call-done), kind=kOutput, calls=%fused_computation.4 | convolution fusion | flops 4371660800 | bytes 10584064 | tf_op jit(solution)/shard_map/dot_general | solution.py:158
  146.7 2.5 copy.24.x_ref
  149.2 9.8 %shard_map.109 = (f32[1024,512]{1,0:T(8,128)}, bf16[1024,256]{1,0:T(8,128)(2,1)}, f32[512,256]{1,0:T(8,128)}, f32[1,256]{1,0:T(1,128)}) custom-call(bf16[1024,1040]{1,0:T(8,128)(2,1)} %copy.24.x_ref, bf16[16,256]{1,0:T(8,128)(2,1)} %up_ref.1, f32[1,256]{1,0:T(1,128)} %bitcast.194, f32[1024,1]{1,0:T(8,128)} %copy.25.shift_ref), custom_call_target="tpu_custom_call" | custom-call | tf_op jit(solution)/shard_map/pallas_call | solution.py:164
  159.0 0.0 all-gather.17.cloned.1.call-update
  159.0 0.0 all-gather.15.cloned.1.call-start
  159.1 0.5 all-gather.15.cloned.1.call-update
  159.6 0.0 all-gather.13.cloned.1.call-start
  159.6 0.7 exponential_bitcast_fusion
  160.3 11.0 %all-gather.1 = f32[8,1,256]{2,1,0:T(1,128)S(1)} all-gather(f32[1,1,256]{2,1,0:T(1,128)S(1)} %exponential_bitcast_fusion), channel_id=1, replica_groups=mesh['sp_0'=8,'sp_1'=8,'tp'=8] {'sp_1'}, dimensions={0}, use_global_device_ids=true | all-gather | bytes 9216 | tf_op jit(solution)/shard_map/all_gather | solution.py:40
  171.3 45.2 %all-gather.17.cloned.1.call-done = f32[4096,256]{1,0:T(8,128)} async-done(((f32[512,256]{1,0:T(8,128)}), f32[4096,256]{1,0:T(8,128)}) %all-gather.17.cloned.1.call-update) | async-done | bytes 4194320 | tf_op jit(solution)/shard_map/all_gather | solution.py:40
  216.6 3.2 bitcast_add_fusion
  219.8 0.0 all-gather.13.cloned.1.call-update
  219.8 78.0 %all-gather.15.cloned.1.call-done = bf16[512,2048]{0,1:T(8,128)(2,1)} async-done(((bf16[512,32]{0,1:T(8,128)(2,1)}), bf16[512,2048]{0,1:T(8,128)(2,1)}) %all-gather.15.cloned.1.call-update) | async-done | bytes 2097168 | tf_op jit(solution)/shard_map/all_gather | solution.py:177
  297.9 3.9 copy.26.out_w_ref
  301.8 11.1 %all-gather.2 = f32[8,1,256]{2,1,0:T(1,128)S(1)} all-gather(f32[1,1,256]{2,1,0:T(1,128)S(1)} %bitcast.183), channel_id=1, replica_groups=mesh['sp_0'=8,'sp_1'=8,'tp'=8] {'sp_0'}, dimensions={0}, use_global_device_ids=true | all-gather | bytes 9216 | tf_op jit(solution)/shard_map/all_gather | solution.py:40
  312.9 46.0 %all-gather.13.cloned.1.call-done = f32[8,512,256]{2,1,0:T(8,128)} async-done(((f32[1,512,256]{2,1,0:T(8,128)}), f32[8,512,256]{2,1,0:T(8,128)}) %all-gather.13.cloned.1.call-update) | async-done | bytes 4194320 | tf_op jit(solution)/shard_map/all_gather | solution.py:40
  359.0 5.0 %fusion.14.carried_ref = bf16[512,256]{1,0:T(8,128)(2,1)} fusion(f32[8,512,256]{2,1,0:T(8,128)} %all-gather.13.cloned.1.call-done, f32[4096,256]{1,0:T(8,128)} %all-gather.17.cloned.1.call-done, f32[256]{0:T(256)S(1)} %bitcast.181, f32[256]{0:T(256)S(1)} %bitcast.179, f32[256]{0:T(256)S(1)} %bitcast.177, f32[256]{0:T(256)S(1)} %bitcast.175, ...), kind=kLoop, calls=%fused_computation.15 | loop fusion | flops 6422528 | bytes 8668176 | tf_op jit(solution)/shard_map/convert_element_type | solution.py:183
  363.9 8.3 %shard_map.110 = bf16[1024,2048]{1,0:T(8,128)(2,1)} custom-call(f32[1024,512]{1,0:T(8,128)} %get-tuple-element.9.att_ref, bf16[1024,256]{1,0:T(8,128)(2,1)} %get-tuple-element.10.far_ref, bf16[512,256]{1,0:T(8,128)(2,1)} %fusion.14.carried_ref, f32[1,512]{1,0:T(1,128)} %bitcast.193, bf16[512,2048]{1,0:T(8,128)(2,1)} %copy.26.out_w_ref), custom_call_target="tpu_custom_call" | custom-call | tf_op jit(solution)/shard_map/pallas_call | solution.py:178
  372.3 53.9 %all_to_all.5 = bf16[8,128,2048]{2,1,0:T(8,128)(2,1)} all-to-all(bf16[8,128,2048]{2,1,0:T(8,128)(2,1)} %bitcast.165), channel_id=1, replica_groups=mesh['sp_0'=8,'sp_1'=8,'tp'=8] {'tp'}, dimensions={0} | all-to-all | bytes 8388608 | tf_op jit(solution)/shard_map/all_to_all | solution.py:57
  426.2 3.8 reduce_sum.22
  (4 shorter events, 0.0 us)
Async XLA Ops:
  6.5 46.7 %all-gather.9.cloned.1.call-start = ((), (), s32[]{:S(2)}) async-start(), calls=%async_computation.1 | async-start | bytes 4718592 | tf_op jit(solution)/shard_map/all_gather | solution.py:159
  9.8 128.8 %all-gather.11.cloned.1.call-start = ((), (), s32[]{:S(2)}) async-start(), calls=%async_computation.2 | async-start | bytes 4259840 | tf_op jit(solution)/shard_map/all_gather | solution.py:22
  11.3 205.3 %all-gather.17.cloned.1.call-start = ((), (), s32[]{:S(2)}) async-start(), calls=%async_computation.5 | async-start | bytes 4718592 | tf_op jit(solution)/shard_map/all_gather | solution.py:40
  159.0 138.9 %all-gather.15.cloned.1.call-start = ((), (), s32[]{:S(2)}) async-start(), calls=%async_computation.4 | async-start | bytes 2129920 | tf_op jit(solution)/shard_map/all_gather | solution.py:177
  159.6 199.4 %all-gather.13.cloned.1.call-start = ((), (), s32[]{:S(2)}) async-start(), calls=%async_computation.3 | async-start | bytes 4718592 | tf_op jit(solution)/shard_map/all_gather | solution.py:40
Sparse Core Ops, SparseCore 0:
  9.9 43.2 all-gather.8
  56.3 82.2 all-gather.10
  159.1 57.3 all-gather.16
  219.5 78.3 all-gather.14
  299.8 59.0 all-gather.12

commit v2 on v1

v2 whole, which is shorter than its diff:
```python
import jax
import jax.numpy as jnp
from jax import lax
from jax.experimental import pallas as pl
from jax.experimental.pallas import tpu as pltpu
from jax.sharding import Mesh
from jax.sharding import PartitionSpec as P

DK = 256
DV = 512
TAU = 16
BLOCK = 64
QUAD = 256
D = 2048
EPS = 1e-06
NY = NZ = 8
NX = 4
SP = ("z", "y")
TP = ("x", "c")
ALL = ("z", "y", "x", "c")
MESH = pl.DeviceIdType.MESH
VMEM = pl.BlockSpec(memory_space=pltpu.VMEM)
BF16 = jnp.bfloat16
F32 = jnp.float32
NN, NT, TN = (((1,), (0,)), ((1,), (1,)), ((0,), (0,)))


def dot(a, b, dims):
    return lax.dot_general(a, b, (dims, ((), ())), preferred_element_type=F32)


def block_masks():
    row = lax.broadcasted_iota(jnp.int32, (QUAD, QUAD), 0)
    col = lax.broadcasted_iota(jnp.int32, (QUAD, QUAD), 1)
    return (row // BLOCK == col // BLOCK) & (col <= row)


def split3(value):
    hi = value.astype(BF16)
    rest = value - hi.astype(F32)
    mid = rest.astype(BF16)
    low = (rest - mid.astype(F32)).astype(BF16)
    return hi, mid, low


def remote(src, dst, send, recv, **device):
    return pltpu.make_async_remote_copy(
        src_ref=src, dst_ref=dst, send_sem=send, recv_sem=recv, device_id=device, device_id_type=MESH
    )


class Spread:
    def __init__(self, buf, at, rows, first, send, recv):
        self.buf, self.rows, self.send, self.recv = buf, rows, send, recv
        self.first, self.second = first, "z" if first == "y" else "y"
        self.at = at
        self.where = {"y": lax.axis_index("y"), "z": lax.axis_index("z")}

    def rest(self):
        return (pl.ds(self.at, self.rows), slice(None))

    def shard(self, along):
        pos = dict(self.where)
        pos[self.first] = along
        return self.buf.at[(pos["z"], pos["y"]) + self.rest()]

    def half(self, line, h):
        part = pl.ds(4 * h, 4)
        lead = (line, part) if self.second == "z" else (part, line)
        return self.buf.at[lead + self.rest()]

    def push(self, d):
        mine = self.where[self.first]
        ref = self.shard(mine)
        return remote(ref, ref, self.send.at[d - 1], self.recv.at[d - 1], **{self.first: lax.rem(mine + d, 8)})

    def start_push(self):
        for d in (1, 7, 2, 6, 3, 5, 4):
            self.push(d).start()

    def wait_push(self):
        mine = self.where[self.first]
        for d in (1, 7, 2, 6, 3, 5, 4):
            ref = self.shard(lax.rem(mine - d + 8, 8))
            remote(ref, ref, self.send.at[d - 1], self.recv.at[d - 1], **{self.first: mine}).wait_recv()

    def hop(self, s, h, way):
        mine = self.where[self.second]
        step = 1 if way == 0 else 7
        line = lax.rem(mine + (8 - step) * (s - 1), 8)
        ref = self.half(line, h)
        i = 7 + way * 7 + 2 * (s - 1) + (h if s < 4 else 0)
        return remote(ref, ref, self.send.at[i], self.recv.at[i], **{self.second: lax.rem(mine + step, 8)})

    def wait_hop(self, s, h, way):
        mine = self.where[self.second]
        step = 1 if way == 0 else 7
        ref = self.half(lax.rem(mine + (8 - step) * s, 8), h)
        i = 7 + way * 7 + 2 * (s - 1) + (h if s < 4 else 0)
        remote(ref, ref, self.send.at[i], self.recv.at[i], **{self.second: mine}).wait_recv()

    def hops(self, s):
        if s < 4:
            return [(0, 0), (1, 1), (1, 0), (0, 1)]
        return [(0, 0), (1, 1)]

    def finish(self):
        self.wait_hop(3, 1, 0)
        self.wait_hop(3, 0, 1)
        self.wait_hop(4, 0, 0)
        self.wait_hop(4, 1, 1)

    def drain(self):
        for d in range(1, 8):
            self.push(d).wait_send()
        for s in range(1, 5):
            for h, way in self.hops(s):
                self.hop(s, h, way).wait_send()


def relay(pieces, s):
    for k in range(4 if s < 4 else 2):
        for p in pieces:
            h, way = p.hops(s)[k]
            if s > 1:
                p.wait_hop(s - 1, h, way)
            p.hop(s, h, way).start()


def layer_kernel(
    tok_ref,
    gain_ref,
    wq_ref,
    wk_ref,
    wv_ref,
    down_ref,
    up_ref,
    bias_ref,
    shift_ref,
    ogain_ref,
    wo_ref,
    out_ref,
    xn,
    wqk,
    wv,
    wo,
    att_ref,
    far_ref,
    state_ref,
    total_ref,
    give,
    decay_out,
    got,
    decays,
    answer,
    carried,
    part,
    other,
    chip,
    ring_l,
    ring_r,
    from_l,
    from_r,
    tok_send,
    tok_recv,
    w_send,
    w_recv,
    scan_send,
    scan_recv,
    rs_send,
    rs_recv,
):
    z, y, x, c = (lax.axis_index(a) for a in ALL)
    sp = z * NY + y
    right, left, mate = lax.rem(x + 1, NX), lax.rem(x + NX - 1, NX), 1 - c

    def peer(d):
        p = lax.rem(sp + d, 64)
        return {"z": lax.div(p, 8), "y": lax.rem(p, 8)}

    barrier = pltpu.get_barrier_semaphore()

    def greet(d, carry):
        pl.semaphore_signal(barrier, inc=1, device_id=peer(d), device_id_type=MESH)
        return carry

    pl.semaphore_signal(barrier, inc=1, device_id={"x": right}, device_id_type=MESH)
    pl.semaphore_signal(barrier, inc=1, device_id={"x": left}, device_id_type=MESH)
    pl.semaphore_signal(barrier, inc=1, device_id={"c": mate}, device_id_type=MESH)
    lax.fori_loop(1, 64, greet, 0)

    wv[z, y] = wv_ref[...]
    wqk[z, y, :, 0:DK] = wq_ref[...]
    wqk[z, y, :, DK : 2 * DK] = wk_ref[...]
    wo[z, y] = wo_ref[...].astype(F32).T.astype(BF16)
    for h in range(2):
        rows = slice(64 * h, 64 * h + 64)
        wide = tok_ref[rows, :].astype(F32)
        normed = wide * lax.rsqrt(jnp.mean(wide * wide, axis=-1, keepdims=True) + EPS) * gain_ref[...]
        xn[x, c, rows, :] = normed.astype(BF16)

    pl.semaphore_wait(barrier, 66)

    value = Spread(wv, 0, 32, "y", w_send.at[0], w_recv.at[0])
    qk = Spread(wqk, 0, 32, "z", w_send.at[1], w_recv.at[1])
    out_a = Spread(wo, 0, 16, "y", w_send.at[2], w_recv.at[2])
    out_b = Spread(wo, 16, 16, "z", w_send.at[3], w_recv.at[3])
    value.start_push()
    qk.start_push()

    def rows_of(xx, h):
        return xn.at[xx, c, pl.ds(64 * h, 64), :]

    def token(i, xx, h, to):
        ref = rows_of(xx, h)
        return remote(ref, ref, tok_send.at[i], tok_recv.at[i], x=to)

    def to_mate(i, xx, h):
        ref = rows_of(xx, h)
        return remote(ref, ref, tok_send.at[i], tok_recv.at[i], c=mate)

    far_x = lax.rem(x + 2, NX)
    sends = [token(0, x, 0, right), token(3, x, 1, left), token(1, x, 1, right), token(4, x, 0, left)]
    for s in sends:
        s.start()
    shares = [to_mate(6, x, 0), to_mate(7, x, 1)]
    for s in shares:
        s.start()

    def arrive(i, xx, h, slot):
        token(i, xx, h, x).wait_recv()
        share = to_mate(slot, xx, h)
        share.start()
        shares.append(share)

    value.wait_push()
    qk.wait_push()
    relay((value, qk), 1)
    arrive(0, left, 0, 8)
    sends.append(token(2, left, 0, right))
    sends[-1].start()
    arrive(3, right, 1, 9)
    sends.append(token(5, right, 1, left))
    sends[-1].start()
    relay((value, qk), 2)
    arrive(1, left, 1, 10)
    arrive(4, right, 0, 11)
    relay((value, qk), 3)
    arrive(2, far_x, 0, 12)
    arrive(5, far_x, 1, 13)
    relay((value, qk), 4)
    out_a.start_push()
    out_b.start_push()
    value.finish()
    qk.finish()
    for i, xx, h in [
        (6, x, 0),
        (7, x, 1),
        (8, left, 0),
        (9, right, 1),
        (10, left, 1),
        (11, right, 0),
        (12, far_x, 0),
        (13, far_x, 1),
    ]:
        ref = xn.at[xx, mate, pl.ds(64 * h, 64), :]
        remote(ref, ref, tok_send.at[i], tok_recv.at[i], c=mate).wait_recv()

    state_ref[...] = jnp.zeros_like(state_ref)
    total_ref[...] = jnp.zeros_like(total_ref)
    nb = QUAD // BLOCK

    def quad(i, carry):
        for s in range(1, 5):

            @pl.when(i == s - 1)
            def _():
                if s == 1:
                    out_a.wait_push()
                    out_b.wait_push()
                relay((out_a, out_b), s)

        at = pl.ds(pl.multiple_of(i * QUAD, QUAD), QUAD)
        rows = xn[i].reshape(QUAD, D)
        joined = dot(rows, wqk[...].reshape(D, 2 * DK), NN).astype(BF16)
        v = dot(rows, wv[...].reshape(D, DV), NN).astype(BF16)
        rank = dot(rows, down_ref[...], NN).astype(BF16)
        causal = block_masks()
        lower = jnp.where(causal, 1.0, 0.0).astype(BF16)
        pre = dot(rank, up_ref[...], NN) + bias_ref[...]
        logs = jnp.minimum(pre, 0.0) - jnp.log1p(jnp.exp(-jnp.abs(pre)))
        ones = jnp.ones((8, DK), BF16)
        shift = shift_ref[pl.ds(i, 1), :]
        shifts = sum(dot(jnp.broadcast_to(t.astype(F32), (8, QUAD)).astype(BF16), ones, TN) for t in split3(shift)) * 0.125
        decay = logs * (1.0 / TAU) + shifts
        hi, mid, low = split3(decay)
        cumul = dot(lower, hi, NN) + (dot(lower, mid, NN) + dot(lower, low, NN))
        cube = cumul.reshape(nb, BLOCK, DK)
        middle, final = (cube[:, BLOCK // 2 : BLOCK // 2 + 1], cube[:, BLOCK - 1 : BLOCK])
        centre = (cube - middle).reshape(QUAD, DK)
        tail = (final - cube).reshape(QUAD, DK)
        q = joined[:, 0:DK].astype(F32) * DK ** (-0.5)
        k = joined[:, DK : 2 * DK].astype(F32)
        q_scaled = (q * jnp.exp(centre)).astype(BF16)
        k_scaled = (k * jnp.exp(-centre)).astype(BF16)
        reach = q * jnp.exp(cumul)
        decayed = (k * jnp.exp(tail)).astype(BF16)
        scores = jnp.where(causal, dot(q_scaled, k_scaled, NT), 0.0).astype(BF16)
        within = dot(scores, v, NN)
        for n in range(nb):
            cut = slice(n * BLOCK, (n + 1) * BLOCK)
            base = total_ref[...]
            rows_at = pl.ds(pl.multiple_of(i * QUAD + n * BLOCK, BLOCK), BLOCK)
            far_ref[rows_at, :] = (reach[cut] * jnp.exp(base)).astype(BF16)
            state = state_ref[...]
            read = dot(reach[cut].astype(BF16), state.astype(BF16), NT)
            att_ref[rows_at, :] = within[cut] + read
            state_ref[...] = jnp.exp(final[n]) * state + dot(v[cut], decayed[cut], TN)
            total_ref[...] = base + final[n]
        return carry

    lax.fori_loop(0, NX, quad, 0)

    give[...] = state_ref[...].reshape(64, 8, DK).astype(BF16)
    decay_out[...] = jnp.exp(total_ref[...])
    got[sp] = give[sp]
    decays[sp] = decay_out[...]

    def ask(d):
        j = lax.rem(sp + d, 64)
        return (
            remote(give.at[j], got.at[sp], scan_send.at[0], scan_recv.at[0], **peer(d)),
            remote(decay_out, decays.at[sp], scan_send.at[1], scan_recv.at[1], **peer(d)),
        )

    def reply(d):
        j = lax.rem(sp + d, 64)
        return remote(answer.at[j], carried.at[sp], scan_send.at[2], scan_recv.at[2], **peer(d))

    def start_ask(d, carry):
        for r in ask(d):
            r.start()
        return carry

    def start_reply(d, carry):
        reply(d).start()
        return carry

    def wait_all(ref, sem):
        most = ref.at[pl.ds(0, 63)]
        pltpu.make_async_copy(most, most, sem).wait()

    lax.fori_loop(1, 64, start_ask, 0)
    wait_all(got, scan_recv.at[0])
    wait_all(decays, scan_recv.at[1])

    def prefix(j, carry):
        answer[j] = carry.astype(BF16)
        return decays[j] * carry + got[j].astype(F32)

    lax.fori_loop(0, 64, prefix, jnp.zeros((8, DK), F32))
    carried[sp] = answer[sp]
    lax.fori_loop(1, 64, start_reply, 0)
    out_a.finish()
    out_b.finish()
    wait_all(carried, scan_recv.at[2])

    halves = (pl.ds(0, 64), pl.ds(64, 64))

    def swap(k):
        return remote(part.at[k, mate], other.at[k], rs_send.at[k], rs_recv.at[k], c=mate)

    def ring(i, src, dst, to):
        return remote(src, dst, rs_send.at[4 + i], rs_recv.at[4 + i], x=to)

    hops = (
        ring(0, chip.at[0, halves[0]], ring_l, right),
        ring(1, chip.at[0, halves[1]], ring_r, left),
        ring(2, chip.at[1, halves[1]], from_l.at[halves[1]], right),
        ring(3, chip.at[2, halves[0]], from_r.at[halves[0]], left),
        ring(4, chip.at[1, halves[0]], from_l.at[halves[0]], right),
        ring(5, chip.at[2, halves[1]], from_r.at[halves[1]], left),
    )

    def both(k, rows):
        return part[k, c, rows, :].astype(F32) + other[k, rows, :].astype(F32)

    def finish(k, carry):
        off = jnp.where(k == 0, 2, jnp.where(k == 1, 1, jnp.where(k == 2, 3, 0)))
        to = lax.rem(x + off, NX)
        at = pl.ds(pl.multiple_of(to * QUAD, QUAD), QUAD)
        att = att_ref[at, :] + dot(far_ref[at, :], carried[...].reshape(DV, DK), NT)
        shaped = att * lax.rsqrt(jnp.mean(att * att, axis=-1, keepdims=True) + EPS) * ogain_ref[...]
        res = dot(shaped.astype(BF16), wo[...].reshape(D, DV), NT).astype(BF16)
        part[k] = res.reshape(2, 128, D)
        swap(k).start()

        @pl.when(k == 1)
        def _():
            swap(0).wait_recv()
            chip[0] = both(0, slice(None)).astype(BF16)
            hops[0].start()
            hops[1].start()

        @pl.when(k == 2)
        def _():
            swap(1).wait_recv()
            chip[1, halves[1], :] = both(1, halves[1]).astype(BF16)
            hops[2].start()

        @pl.when(k == 3)
        def _():
            swap(2).wait_recv()
            chip[2, halves[0], :] = both(2, halves[0]).astype(BF16)
            hops[3].start()

        return carry

    lax.fori_loop(0, NX, finish, 0)
    hops[0].wait_recv()
    chip[1, halves[0], :] = (both(1, halves[0]) + ring_l[...].astype(F32)).astype(BF16)
    hops[4].start()
    hops[1].wait_recv()
    chip[2, halves[1], :] = (both(2, halves[1]) + ring_r[...].astype(F32)).astype(BF16)
    hops[5].start()
    swap(3).wait_recv()
    for i in (2, 3, 4, 5):
        hops[i].wait_recv()
    out_ref[...] = (both(3, slice(None)) + from_l[...].astype(F32) + from_r[...].astype(F32)).astype(BF16)

    for s in sends + shares:
        s.wait_send()
    for p in (value, qk, out_a, out_b):
        p.drain()
    sent = give.at[pl.ds(0, 63)]
    pltpu.make_async_copy(sent, sent, scan_send.at[0]).wait()
    wait_all(decays, scan_send.at[1])
    wait_all(answer, scan_send.at[2])
    for k in range(4):
        swap(k).wait_send()
    for h in hops:
        h.wait_send()


def on_device(
    tokens,
    norm_gain,
    w_query,
    w_key,
    w_value,
    w_rank_down,
    w_rank_up,
    gate_bias,
    decay_shift,
    out_gain,
    w_out,
):
    return pl.pallas_call(
        layer_kernel,
        out_shape=jax.ShapeDtypeStruct(tokens.shape, BF16),
        in_specs=[VMEM] * 11,
        out_specs=VMEM,
        scratch_shapes=[
            pltpu.VMEM((NX, 2, 128, D), BF16),
            pltpu.VMEM((NZ, NY, 32, 2 * DK), BF16),
            pltpu.VMEM((NZ, NY, 32, DV), BF16),
            pltpu.VMEM((NZ, NY, 32, DV), BF16),
            pltpu.VMEM((1024, DV), F32),
            pltpu.VMEM((1024, DK), BF16),
            pltpu.VMEM((DV, DK), F32),
            pltpu.VMEM((1, DK), F32),
            pltpu.VMEM((64, 8, DK), BF16),
            pltpu.VMEM((1, DK), F32),
            pltpu.VMEM((64, 8, DK), BF16),
            pltpu.VMEM((64, 1, DK), F32),
            pltpu.VMEM((64, 8, DK), BF16),
            pltpu.VMEM((64, 8, DK), BF16),
            pltpu.VMEM((NX, 2, 128, D), BF16),
            pltpu.VMEM((NX, 128, D), BF16),
            pltpu.VMEM((3, 128, D), BF16),
            pltpu.VMEM((64, D), BF16),
            pltpu.VMEM((64, D), BF16),
            pltpu.VMEM((128, D), BF16),
            pltpu.VMEM((128, D), BF16),
            pltpu.SemaphoreType.DMA((14,)),
            pltpu.SemaphoreType.DMA((14,)),
            pltpu.SemaphoreType.DMA((4, 21)),
            pltpu.SemaphoreType.DMA((4, 21)),
            pltpu.SemaphoreType.DMA((3,)),
            pltpu.SemaphoreType.DMA((3,)),
            pltpu.SemaphoreType.DMA((10,)),
            pltpu.SemaphoreType.DMA((10,)),
        ],
        compiler_params=pltpu.CompilerParams(
            collective_id=0, has_side_effects=True, vmem_limit_bytes=56 * 1024 * 1024
        ),
    )(
        tokens,
        norm_gain[None],
        w_query,
        w_key,
        w_value,
        w_rank_down,
        w_rank_up,
        gate_bias[None],
        decay_shift.reshape(NX, QUAD),
        out_gain[None],
        w_out,
    )


def solution(mesh):
    finer = Mesh(mesh.devices.reshape(NZ, NY, NX, 2), ALL)
    in_specs = (
        P(ALL, None),
        P(),
        P(SP, TP),
        P(SP, TP),
        P(SP, TP),
        P(),
        P(None, TP),
        P(TP),
        P(SP),
        P(),
        P(TP, SP),
    )
    return jax.shard_map(on_device, mesh=finer, in_specs=in_specs, out_specs=P(ALL, None), check_vma=False)
```

time: 437 us -> 118 us (0.27)
  waiting for transfers between devices: 294 us -> 0 us
  Pallas kernels: 18.1 us -> 112 us
  blocking collectives: 76 us -> 0 us
  other arithmetic: 16.7 us -> 0 us
  between operations: 13.2 us -> 0.01 us
  matrix products: 8.09 us -> 0 us
    all_gather x5 -> x0, waiting for transfers between devices: 294 us -> none  [the longest x2 91.3 us: entering(): pieces = jax.tree.map(lambda part: lax.all_gather(part, axis), total)]
    pallas_call x2 -> x1, Pallas kernels: 18.1 us -> 112 us  [on_device(): pl.pallas_call(layer_kernel, out_shape=jax.ShapeDtypeStruct(tokens.shape,...]
    all_to_all x1 -> x0, blocking collectives: 53.9 us -> none  [sent_and_summed(): parts = lax.all_to_all(cut_along(value, dim, size), axis, 0, 0, tiled=True)]
    all_gather x2 -> x0, blocking collectives: 22.1 us -> none  [entering(): pieces = jax.tree.map(lambda part: lax.all_gather(part, axis), total)]
    dot_general x1 -> x0, matrix products: 8.09 us -> none  [on_device(): jnp.dot(lax.all_gather(normed, 'tp', axis=0, tiled=True), w_joined, prefe...]
    convert_element_type x2 -> x0, other arithmetic: 6.99 us -> none  [the longest x1 4.96 us: on_device(): carried.astype(jnp.bfloat16)]
    reduce_sum x2 -> x0, other arithmetic: 5.08 us -> none  [the longest x1 3.85 us: sent_and_summed(): return jnp.sum(parts.astype(jnp.float32), axis=0)]
  transfers between devices with their start and end apart: 5 -> 0, of which waited for: 5 -> 0; matrix products, arithmetic and copies ran while one was open for 3% -> 0% of each run, Pallas kernels for 0% -> 0%
where the time goes in v2:
time: 118 us
  Pallas kernels  112 us (95%)
  local copies, waits for them, and re-layouts  5.71 us (5%)
    pallas_call x1, Pallas kernels, on_device(): pl.pallas_call(layer_kernel, out_shape=jax.ShapeDtypeStruct(tokens.shape,...  112 us
    unnamed x7, local copies, waits for them, and re-layouts  5.12 us

profile of v2, /device:TPU:1, one launch (start us, length us, event | category | flops | bytes accessed | tf_op | source)
XLA Modules:
  0.0 118.2 jit_solution(3501333374635144213)
XLA Ops:
  0.0 0.0 copy-start.1
  0.0 0.7 copy-done.1
  0.7 0.6 reshape.3.shift_ref
  1.3 0.0 copy-start
  1.3 1.5 %copy.13.wo_ref = bf16[512,32]{1,0:T(8,128)(2,1)} copy(bf16[512,32]{0,1:T(8,128)(2,1)} %param.21) | data formatting | bytes 65536 | tf_op args[10]
  2.8 0.0 copy-done
  2.8 1.0 copy.12.down_ref
  3.8 112.4 %shard_map.109 = bf16[128,2048]{1,0:T(8,128)(2,1)} custom-call(bf16[128,2048]{1,0:T(8,128)(2,1)} %tok_ref.1, f32[1,2048]{1,0:T(1,128)} %bitcast.3, bf16[32,256]{1,0:T(8,128)(2,1)} %wq_ref.1, bf16[32,256]{1,0:T(8,128)(2,1)} %wk_ref.1, bf16[32,512]{1,0:T(8,128)(2,1)} %wv_ref.1, bf16[2048,16]{1,0:T(8,128)(2,1)} %copy.12.down_ref, bf16[16,256]{1,0:T(8,128)(2,1)} %up_ref.1, ...), custom_call_target="tpu_custom_call" | custom-call | tf_op jit(solution)/shard_map/pallas_call | solution.py:458
  116.3 1.9 %copy.15 = bf16[128,2048]{1,0:T(8,128)(2,1)} copy(bf16[128,2048]{1,0:T(8,128)(2,1)} %shard_map.109) | data formatting | bytes 1048576
Async XLA Ops:
  0.0 0.7 copy-start.1
  1.3 1.5 %copy-start = (bf16[2048,16]{0,1:T(8,128)(2,1)S(1)}, bf16[2048,16]{0,1:T(8,128)(2,1)}, u32[]{:S(2)}) copy-start(bf16[2048,16]{0,1:T(8,128)(2,1)} %param.16) | copy-start | bytes 196612

commit v3 on v2

--- a/solution.py
+++ b/solution.py
@@ -20,6 +20,7 @@
 ALL = ("z", "y", "x", "c")
 MESH = pl.DeviceIdType.MESH
 VMEM = pl.BlockSpec(memory_space=pltpu.VMEM)
+ANY = pl.BlockSpec(memory_space=pl.ANY)
 BF16 = jnp.bfloat16
 F32 = jnp.float32
 NN, NT, TN = (((1,), (0,)), ((1,), (1,)), ((0,), (0,)))
@@ -29,10 +30,8 @@
     return lax.dot_general(a, b, (dims, ((), ())), preferred_element_type=F32)
 
 
-def block_masks():
-    row = lax.broadcasted_iota(jnp.int32, (QUAD, QUAD), 0)
-    col = lax.broadcasted_iota(jnp.int32, (QUAD, QUAD), 1)
-    return (row // BLOCK == col // BLOCK) & (col <= row)
+def positions():
+    return (lax.broadcasted_iota(jnp.int32, (QUAD, QUAD), i) for i in range(2))
 
 
 def split3(value):
@@ -118,36 +117,90 @@
                 self.hop(s, h, way).wait_send()
 
 
+class FineSpread(Spread):
+    def half(self, line, h):
+        pair = lax.rem(lax.div(self.where[self.first], 2) + h, 4)
+        part = pl.ds(2 * pair, 2)
+        lead = (line, part) if self.second == "z" else (part, line)
+        return self.buf.at[lead + self.rest()]
+
+    def wait_from(self, d):
+        mine = self.where[self.first]
+        ref = self.shard(lax.rem(mine - d + 8, 8))
+        remote(ref, ref, self.send.at[d - 1], self.recv.at[d - 1], **{self.first: mine}).wait_recv()
+
+    def wait_pair(self, h):
+        mine = self.where[self.first]
+        odd = lax.rem(mine, 2)
+        if h == 0:
+            self.wait_from(7 - 6 * odd)
+        else:
+            for d in range(2):
+                self.wait_from(lax.rem(8 - 2 * h + odd - d, 8))
+
+    def index(self, s, h, way):
+        return 7 + 14 * way + 4 * (s - 1) + (h if s < 4 else h // 2)
+
+    def hop(self, s, h, way):
+        mine = self.where[self.second]
+        step = 1 if way == 0 else 7
+        ref = self.half(lax.rem(mine + (8 - step) * (s - 1), 8), h)
+        i = self.index(s, h, way)
+        return remote(ref, ref, self.send.at[i], self.recv.at[i], **{self.second: lax.rem(mine + step, 8)})
+
+    def wait_hop(self, s, h, way):
+        mine = self.where[self.second]
+        step = 1 if way == 0 else 7
+        ref = self.half(lax.rem(mine + (8 - step) * s, 8), h)
+        i = self.index(s, h, way)
+        remote(ref, ref, self.send.at[i], self.recv.at[i], **{self.second: mine}).wait_recv()
+
+    def hops(self, s):
+        both = [(0, 0), (0, 1), (1, 0), (1, 1), (3, 0), (3, 1), (2, 0), (2, 1)]
+        return both if s < 4 else [(0, 0), (1, 1), (2, 0), (3, 1)]
+
+    def finish(self):
+        for h in range(4):
+            self.wait_hop(3, h, 1 - h % 2)
+            self.wait_hop(4, h, h % 2)
+
+
 def relay(pieces, s):
-    for k in range(4 if s < 4 else 2):
+    for k in range(len(pieces[0].hops(s))):
         for p in pieces:
             h, way = p.hops(s)[k]
             if s > 1:
                 p.wait_hop(s - 1, h, way)
+            elif way == 0 and isinstance(p, FineSpread):
+                p.wait_pair(h)
             p.hop(s, h, way).start()
 
 
 def layer_kernel(
-    tok_ref,
+    tok_hbm,
     gain_ref,
-    wq_ref,
-    wk_ref,
-    wv_ref,
+    wq_hbm,
+    wk_hbm,
+    wv_hbm,
     down_ref,
     up_ref,
     bias_ref,
     shift_ref,
     ogain_ref,
-    wo_ref,
+    wo_hbm,
     out_ref,
+    tok_ref,
     xn,
-    wqk,
-    wv,
+    wkv,
+    wqb,
     wo,
+    kv_ref,
+    cum_ref,
+    base_ref,
+    starts,
     att_ref,
     far_ref,
     state_ref,
-    total_ref,
     give,
     decay_out,
     got,
@@ -161,8 +214,11 @@
     ring_r,
     from_l,
     from_r,
+    in_sem,
     tok_send,
     tok_recv,
+    kv_send,
+    kv_recv,
     w_send,
     w_recv,
     scan_send,
@@ -179,163 +235,167 @@
         return {"z": lax.div(p, 8), "y": lax.rem(p, 8)}
 
     barrier = pltpu.get_barrier_semaphore()
-
-    def greet(d, carry):
-        pl.semaphore_signal(barrier, inc=1, device_id=peer(d), device_id_type=MESH)
-        return carry
-
-    pl.semaphore_signal(barrier, inc=1, device_id={"x": right}, device_id_type=MESH)
-    pl.semaphore_signal(barrier, inc=1, device_id={"x": left}, device_id_type=MESH)
-    pl.semaphore_signal(barrier, inc=1, device_id={"c": mate}, device_id_type=MESH)
-    lax.fori_loop(1, 64, greet, 0)
-
-    wv[z, y] = wv_ref[...]
-    wqk[z, y, :, 0:DK] = wq_ref[...]
-    wqk[z, y, :, DK : 2 * DK] = wk_ref[...]
-    wo[z, y] = wo_ref[...].astype(F32).T.astype(BF16)
-    for h in range(2):
+    near = [{"x": right}, {"x": left}, {"c": mate}]
+    near += [{a: lax.rem(i + d, 8)} for a, i in (("y", y), ("z", z)) for d in range(1, 8)]
+    for device in near:
+        pl.semaphore_signal(barrier, inc=1, device_id=device, device_id_type=MESH)
+
+    loads = (
+        pltpu.make_async_copy(wk_hbm, wkv.at[z, y, :, pl.ds(0, DK)], in_sem.at[0]),
+        pltpu.make_async_copy(wv_hbm, wkv.at[z, y, :, pl.ds(DK, DV)], in_sem.at[1]),
+        pltpu.make_async_copy(tok_hbm.at[pl.ds(0, 64)], tok_ref.at[pl.ds(0, 64)], in_sem.at[2]),
+        pltpu.make_async_copy(tok_hbm.at[pl.ds(64, 64)], tok_ref.at[pl.ds(64, 64)], in_sem.at[3]),
+        pltpu.make_async_copy(wq_hbm, wqb.at[z, y], in_sem.at[4]),
+        pltpu.make_async_copy(wo_hbm, wo.at[z, y], in_sem.at[5]),
+    )
+    for load in loads:
+        load.start()
+
+    kv = tuple(FineSpread(wkv, 16 * i, 16, "yz"[i], kv_send.at[i], kv_recv.at[i]) for i in range(2))
+    qs = tuple(Spread(wqb, 16 * i, 16, "yz"[i], w_send.at[i], w_recv.at[i]) for i in range(2))
+    outs = tuple(Spread(wo, 16 * i, 16, "yz"[i], w_send.at[2 + i], w_recv.at[2 + i]) for i in range(2))
+
+    def start_push(pieces):
+        for p in pieces:
+            p.start_push()
+
+    def wait_push(pieces):
+        for p in pieces:
+            p.wait_push()
+
+    def rows_of(xx, h):
+        return xn.at[xx, c, pl.ds(64 * h, 64), :]
+
+    def token(i, xx, h, to):
+        ref = rows_of(xx, h)
+        return remote(ref, ref, tok_send.at[i], tok_recv.at[i], x=to)
+
+    def to_mate(i, xx, h):
+        ref = rows_of(xx, h)
+        return remote(ref, ref, tok_send.at[i], tok_recv.at[i], c=mate)
+
+    def norm(h):
         rows = slice(64 * h, 64 * h + 64)
         wide = tok_ref[rows, :].astype(F32)
         normed = wide * lax.rsqrt(jnp.mean(wide * wide, axis=-1, keepdims=True) + EPS) * gain_ref[...]
         xn[x, c, rows, :] = normed.astype(BF16)
 
-    pl.semaphore_wait(barrier, 66)
-
-    value = Spread(wv, 0, 32, "y", w_send.at[0], w_recv.at[0])
-    qk = Spread(wqk, 0, 32, "z", w_send.at[1], w_recv.at[1])
-    out_a = Spread(wo, 0, 16, "y", w_send.at[2], w_recv.at[2])
-    out_b = Spread(wo, 16, 16, "z", w_send.at[3], w_recv.at[3])
-    value.start_push()
-    qk.start_push()
-
-    def rows_of(xx, h):
-        return xn.at[xx, c, pl.ds(64 * h, 64), :]
-
-    def token(i, xx, h, to):
-        ref = rows_of(xx, h)
-        return remote(ref, ref, tok_send.at[i], tok_recv.at[i], x=to)
-
-    def to_mate(i, xx, h):
-        ref = rows_of(xx, h)
-        return remote(ref, ref, tok_send.at[i], tok_recv.at[i], c=mate)
-
     far_x = lax.rem(x + 2, NX)
-    sends = [token(0, x, 0, right), token(3, x, 1, left), token(1, x, 1, right), token(4, x, 0, left)]
-    for s in sends:
-        s.start()
-    shares = [to_mate(6, x, 0), to_mate(7, x, 1)]
-    for s in shares:
-        s.start()
+    sends = []
+
+    def go(copy):
+        copy.start()
+        sends.append(copy)
 
     def arrive(i, xx, h, slot):
         token(i, xx, h, x).wait_recv()
-        share = to_mate(slot, xx, h)
-        share.start()
-        shares.append(share)
-
-    value.wait_push()
-    qk.wait_push()
-    relay((value, qk), 1)
-    arrive(0, left, 0, 8)
-    sends.append(token(2, left, 0, right))
-    sends[-1].start()
-    arrive(3, right, 1, 9)
-    sends.append(token(5, right, 1, left))
-    sends[-1].start()
-    relay((value, qk), 2)
-    arrive(1, left, 1, 10)
-    arrive(4, right, 0, 11)
-    relay((value, qk), 3)
-    arrive(2, far_x, 0, 12)
-    arrive(5, far_x, 1, 13)
-    relay((value, qk), 4)
-    out_a.start_push()
-    out_b.start_push()
-    value.finish()
-    qk.finish()
-    for i, xx, h in [
-        (6, x, 0),
-        (7, x, 1),
-        (8, left, 0),
-        (9, right, 1),
-        (10, left, 1),
-        (11, right, 0),
-        (12, far_x, 0),
-        (13, far_x, 1),
-    ]:
+        go(to_mate(slot, xx, h))
+
+    def from_mate(i, xx, h):
         ref = xn.at[xx, mate, pl.ds(64 * h, 64), :]
         remote(ref, ref, tok_send.at[i], tok_recv.at[i], c=mate).wait_recv()
 
-    state_ref[...] = jnp.zeros_like(state_ref)
-    total_ref[...] = jnp.zeros_like(total_ref)
-    nb = QUAD // BLOCK
-
-    def quad(i, carry):
-        for s in range(1, 5):
-
-            @pl.when(i == s - 1)
-            def _():
-                if s == 1:
-                    out_a.wait_push()
-                    out_b.wait_push()
-                relay((out_a, out_b), s)
-
-        at = pl.ds(pl.multiple_of(i * QUAD, QUAD), QUAD)
-        rows = xn[i].reshape(QUAD, D)
-        joined = dot(rows, wqk[...].reshape(D, 2 * DK), NN).astype(BF16)
-        v = dot(rows, wv[...].reshape(D, DV), NN).astype(BF16)
-        rank = dot(rows, down_ref[...], NN).astype(BF16)
-        causal = block_masks()
-        lower = jnp.where(causal, 1.0, 0.0).astype(BF16)
+    row, col = positions()
+    lower = jnp.where(col <= row, 1.0, 0.0).astype(BF16)
+
+    def gates(i):
+        rank = dot(xn[i].reshape(QUAD, D), down_ref[...], NT).astype(BF16)
         pre = dot(rank, up_ref[...], NN) + bias_ref[...]
         logs = jnp.minimum(pre, 0.0) - jnp.log1p(jnp.exp(-jnp.abs(pre)))
         ones = jnp.ones((8, DK), BF16)
-        shift = shift_ref[pl.ds(i, 1), :]
+        shift = shift_ref[:, pl.ds(pl.multiple_of(i * QUAD, QUAD), QUAD)]
         shifts = sum(dot(jnp.broadcast_to(t.astype(F32), (8, QUAD)).astype(BF16), ones, TN) for t in split3(shift)) * 0.125
-        decay = logs * (1.0 / TAU) + shifts
-        hi, mid, low = split3(decay)
-        cumul = dot(lower, hi, NN) + (dot(lower, mid, NN) + dot(lower, low, NN))
-        cube = cumul.reshape(nb, BLOCK, DK)
-        middle, final = (cube[:, BLOCK // 2 : BLOCK // 2 + 1], cube[:, BLOCK - 1 : BLOCK])
-        centre = (cube - middle).reshape(QUAD, DK)
-        tail = (final - cube).reshape(QUAD, DK)
-        q = joined[:, 0:DK].astype(F32) * DK ** (-0.5)
-        k = joined[:, DK : 2 * DK].astype(F32)
-        q_scaled = (q * jnp.exp(centre)).astype(BF16)
-        k_scaled = (k * jnp.exp(-centre)).astype(BF16)
-        reach = q * jnp.exp(cumul)
-        decayed = (k * jnp.exp(tail)).astype(BF16)
-        scores = jnp.where(causal, dot(q_scaled, k_scaled, NT), 0.0).astype(BF16)
-        within = dot(scores, v, NN)
-        for n in range(nb):
-            cut = slice(n * BLOCK, (n + 1) * BLOCK)
-            base = total_ref[...]
-            rows_at = pl.ds(pl.multiple_of(i * QUAD + n * BLOCK, BLOCK), BLOCK)
-            far_ref[rows_at, :] = (reach[cut] * jnp.exp(base)).astype(BF16)
-            state = state_ref[...]
-            read = dot(reach[cut].astype(BF16), state.astype(BF16), NT)
-            att_ref[rows_at, :] = within[cut] + read
-            state_ref[...] = jnp.exp(final[n]) * state + dot(v[cut], decayed[cut], TN)
-            total_ref[...] = base + final[n]
+        hi, mid, low = split3(logs * (1.0 / TAU) + shifts)
+        cum_ref[i] = dot(lower, hi, NN) + (dot(lower, mid, NN) + dot(lower, low, NN))
+
+    loads[0].wait()
+    loads[1].wait()
+    pl.semaphore_wait(barrier, 17)
+    start_push(kv)
+    loads[2].wait()
+    norm(0)
+    go(token(0, x, 0, right))
+    go(to_mate(6, x, 0))
+    loads[3].wait()
+    norm(1)
+    go(token(3, x, 1, left))
+    go(to_mate(7, x, 1))
+    go(token(1, x, 1, right))
+    go(token(4, x, 0, left))
+    relay(kv, 1)
+    from_mate(6, x, 0)
+    from_mate(7, x, 1)
+    gates(x)
+    arrive(0, left, 0, 8)
+    go(token(2, left, 0, right))
+    arrive(3, right, 1, 9)
+    go(token(5, right, 1, left))
+    relay(kv, 2)
+    relay(kv, 3)
+    arrive(1, left, 1, 10)
+    arrive(4, right, 0, 11)
+    relay(kv, 4)
+    loads[4].wait()
+    start_push(qs)
+    loads[5].wait()
+    start_push(outs)
+    from_mate(8, left, 0)
+    from_mate(10, left, 1)
+    gates(left)
+    from_mate(9, right, 1)
+    from_mate(11, right, 0)
+    gates(right)
+    arrive(2, far_x, 0, 12)
+    arrive(5, far_x, 1, 13)
+    from_mate(12, far_x, 0)
+    from_mate(13, far_x, 1)
+    gates(far_x)
+    base = jnp.zeros((1, DK), F32)
+    for i in range(NX):
+        base_ref[i] = base
+        base = base + cum_ref[i, QUAD - 1 : QUAD]
+    decay_out[...] = jnp.exp(base)
+    for p in kv:
+        p.finish()
+
+    state_ref[...] = jnp.zeros_like(state_ref)
+
+    def absorb(i, carry):
+        @pl.when(i == 1)
+        def _():
+            wait_push(qs)
+            relay(qs, 1)
+
+        @pl.when(i == 3)
+        def _():
+            relay(qs, 2)
+
+        now = dot(xn[i].reshape(QUAD, D), wkv[...].reshape(D, DK + DV), NN).astype(BF16)
+        kv_ref[pl.ds(pl.multiple_of(i * QUAD, QUAD), QUAD), :] = now
+        cum = cum_ref[i]
+        final = cum[QUAD - 1 : QUAD]
+        decayed = (now[:, 0:DK].astype(F32) * jnp.exp(final - cum)).astype(BF16)
+        state = state_ref[...]
+        starts[i] = state.astype(BF16)
+        state_ref[...] = jnp.exp(final) * state + dot(now[:, DK:], decayed, TN)
         return carry
 
-    lax.fori_loop(0, NX, quad, 0)
+    lax.fori_loop(0, NX, absorb, 0)
 
     give[...] = state_ref[...].reshape(64, 8, DK).astype(BF16)
-    decay_out[...] = jnp.exp(total_ref[...])
-    got[sp] = give[sp]
-    decays[sp] = decay_out[...]
 
     def ask(d):
-        j = lax.rem(sp + d, 64)
+        p = peer(d)
+        j = p["z"] * NY + p["y"]
         return (
-            remote(give.at[j], got.at[sp], scan_send.at[0], scan_recv.at[0], **peer(d)),
-            remote(decay_out, decays.at[sp], scan_send.at[1], scan_recv.at[1], **peer(d)),
+            remote(give.at[j], got.at[sp], scan_send.at[0], scan_recv.at[0], **p),
+            remote(decay_out, decays.at[sp], scan_send.at[1], scan_recv.at[1], **p),
         )
 
     def reply(d):
-        j = lax.rem(sp + d, 64)
-        return remote(answer.at[j], carried.at[sp], scan_send.at[2], scan_recv.at[2], **peer(d))
+        p = peer(d)
+        j = p["z"] * NY + p["y"]
+        return remote(answer.at[j], carried.at[sp], scan_send.at[2], scan_recv.at[2], **p)
 
     def start_ask(d, carry):
         for r in ask(d):
@@ -351,6 +411,43 @@
         pltpu.make_async_copy(most, most, sem).wait()
 
     lax.fori_loop(1, 64, start_ask, 0)
+    got[sp] = give[sp]
+    decays[sp] = decay_out[...]
+    relay(qs, 3)
+    wait_push(outs)
+    relay(outs, 1)
+    relay(qs, 4)
+    relay(outs, 2)
+    for p in qs:
+        p.finish()
+    relay(outs, 3)
+
+    def attend(i, carry):
+        at = pl.ds(pl.multiple_of(i * QUAD, QUAD), QUAD)
+        q = dot(xn[i].reshape(QUAD, D), wqb[...].reshape(D, DK), NN).astype(BF16).astype(F32) * DK ** (-0.5)
+        k = kv_ref[at, 0:DK].astype(F32)
+        v = kv_ref[at, DK : DK + DV]
+        cum = cum_ref[i]
+        cube = cum.reshape(QUAD // BLOCK, BLOCK, DK)
+        centre = (cube - cube[:, BLOCK // 2 : BLOCK // 2 + 1]).reshape(QUAD, DK)
+        q_scaled = (q * jnp.exp(centre)).astype(BF16)
+        k_scaled = (k * jnp.exp(-centre)).astype(BF16)
+        causal = (row // BLOCK == col // BLOCK) & (col <= row)
+        scores = jnp.where(causal, dot(q_scaled, k_scaled, NT), 0.0)
+        lines = [scores[0:BLOCK]]
+        for n in range(1, QUAD // BLOCK):
+            cut = n * BLOCK
+            edge = cum[cut - 1 : cut]
+            q_part = (q[cut : cut + BLOCK] * jnp.exp(cum[cut : cut + BLOCK] - edge)).astype(BF16)
+            k_part = (k[0:cut] * jnp.exp(edge - cum[0:cut])).astype(BF16)
+            k_part = jnp.concatenate([k_part, jnp.zeros((QUAD - cut, DK), BF16)], axis=0)
+            lines.append(scores[cut : cut + BLOCK] + dot(q_part, k_part, NT))
+        scores = jnp.concatenate(lines, axis=0).astype(BF16)
+        reach = q * jnp.exp(cum)
+        att_ref[at, :] = dot(scores, v, NN) + dot(reach.astype(BF16), starts[i], NT)
+        far_ref[at, :] = (reach * jnp.exp(base_ref[i])).astype(BF16)
+        return carry
+
     wait_all(got, scan_recv.at[0])
     wait_all(decays, scan_recv.at[1])
 
@@ -359,10 +456,12 @@
         return decays[j] * carry + got[j].astype(F32)
 
     lax.fori_loop(0, 64, prefix, jnp.zeros((8, DK), F32))
+    lax.fori_loop(1, 64, start_reply, 0)
+    relay(outs, 4)
+    lax.fori_loop(0, NX, attend, 0)
     carried[sp] = answer[sp]
-    lax.fori_loop(1, 64, start_reply, 0)
-    out_a.finish()
-    out_b.finish()
+    for p in outs:
+        p.finish()
     wait_all(carried, scan_recv.at[2])
 
     halves = (pl.ds(0, 64), pl.ds(64, 64))
@@ -428,9 +527,9 @@
         hops[i].wait_recv()
     out_ref[...] = (both(3, slice(None)) + from_l[...].astype(F32) + from_r[...].astype(F32)).astype(BF16)
 
-    for s in sends + shares:
+    for s in sends:
         s.wait_send()
-    for p in (value, qk, out_a, out_b):
+    for p in kv + qs + outs:
         p.drain()
     sent = give.at[pl.ds(0, 63)]
     pltpu.make_async_copy(sent, sent, scan_send.at[0]).wait()
@@ -458,17 +557,21 @@
     return pl.pallas_call(
         layer_kernel,
         out_shape=jax.ShapeDtypeStruct(tokens.shape, BF16),
-        in_specs=[VMEM] * 11,
+        in_specs=[ANY, VMEM, ANY, ANY, ANY, VMEM, VMEM, VMEM, VMEM, VMEM, ANY],
         out_specs=VMEM,
         scratch_shapes=[
+            pltpu.VMEM((128, D), BF16),
             pltpu.VMEM((NX, 2, 128, D), BF16),
-            pltpu.VMEM((NZ, NY, 32, 2 * DK), BF16),
+            pltpu.VMEM((NZ, NY, 32, DK + DV), BF16),
+            pltpu.VMEM((NZ, NY, 32, DK), BF16),
             pltpu.VMEM((NZ, NY, 32, DV), BF16),
-            pltpu.VMEM((NZ, NY, 32, DV), BF16),
-            pltpu.VMEM((1024, DV), F32),
-            pltpu.VMEM((1024, DK), BF16),
+            pltpu.VMEM((NX * QUAD, DK + DV), BF16),
+            pltpu.VMEM((NX, QUAD, DK), F32),
+            pltpu.VMEM((NX, 1, DK), F32),
+            pltpu.VMEM((NX, DV, DK), BF16),
+            pltpu.VMEM((NX * QUAD, DV), F32),
+            pltpu.VMEM((NX * QUAD, DK), BF16),
             pltpu.VMEM((DV, DK), F32),
-            pltpu.VMEM((1, DK), F32),
             pltpu.VMEM((64, 8, DK), BF16),
             pltpu.VMEM((1, DK), F32),
             pltpu.VMEM((64, 8, DK), BF16),
@@ -482,8 +585,11 @@
             pltpu.VMEM((64, D), BF16),
             pltpu.VMEM((128, D), BF16),
             pltpu.VMEM((128, D), BF16),
+            pltpu.SemaphoreType.DMA((6,)),
             pltpu.SemaphoreType.DMA((14,)),
             pltpu.SemaphoreType.DMA((14,)),
+            pltpu.SemaphoreType.DMA((2, 35)),
+            pltpu.SemaphoreType.DMA((2, 35)),
             pltpu.SemaphoreType.DMA((4, 21)),
             pltpu.SemaphoreType.DMA((4, 21)),
             pltpu.SemaphoreType.DMA((3,)),
@@ -500,12 +606,12 @@
         w_query,
         w_key,
         w_value,
-        w_rank_down,
+        w_rank_down.T,
         w_rank_up,
         gate_bias[None],
-        decay_shift.reshape(NX, QUAD),
+        decay_shift[None],
         out_gain[None],
-        w_out,
+        w_out.T,
     )
 
 

time: 118 us -> 108 us (0.915)
  Pallas kernels: 112 us -> 106 us
  local copies, waits for them, and re-layouts: 5.71 us -> 1.88 us
    pallas_call x1, Pallas kernels: 112 us -> 106 us  [on_device(): pl.pallas_call(layer_kernel, out_shape=jax.ShapeDtypeStruct(tokens.shape,...]
    unnamed x7 -> x1, local copies, waits for them, and re-layouts: 5.12 us -> 1.88 us
where the time goes in v3:
time: 108 us; the launch traced here: 107 us
  Pallas kernels  106 us (98%)
  local copies, waits for them, and re-layouts  1.88 us (2%)
    pallas_call x1, Pallas kernels, on_device(): pl.pallas_call(layer_kernel, out_shape=jax.ShapeDtypeStruct(tokens.shape,...  106 us

profile of v3, /device:TPU:1, one launch (start us, length us, event | category | flops | bytes accessed | tf_op | source)
XLA Modules:
  0.0 107.5 jit_solution(13104709126300617719)
XLA Ops:
  0.0 105.6 %shard_map.109 = bf16[128,2048]{1,0:T(8,128)(2,1)} custom-call(bf16[128,2048]{1,0:T(8,128)(2,1)} %tok_hbm.1, f32[1,2048]{1,0:T(1,128)} %bitcast.8, bf16[32,256]{1,0:T(8,128)(2,1)} %wq_hbm.1, bf16[32,256]{1,0:T(8,128)(2,1)} %wk_hbm.1, bf16[32,512]{1,0:T(8,128)(2,1)} %wv_hbm.1, bf16[16,2048]{1,0:T(8,128)(2,1)} %bitcast.6, bf16[16,256]{1,0:T(8,128)(2,1)} %up_ref.1, ...), custom_call_target="tpu_custom_call" | custom-call | tf_op jit(solution)/shard_map/pallas_call | solution.py:557
  105.6 1.9 %copy.13 = bf16[128,2048]{1,0:T(8,128)(2,1)} copy(bf16[128,2048]{1,0:T(8,128)(2,1)} %shard_map.109) | data formatting | bytes 1048576

commit v4 on v3

--- a/solution.py
+++ b/solution.py
@@ -20,7 +20,7 @@
 ALL = ("z", "y", "x", "c")
 MESH = pl.DeviceIdType.MESH
 VMEM = pl.BlockSpec(memory_space=pltpu.VMEM)
-ANY = pl.BlockSpec(memory_space=pl.ANY)
+HBM = pl.BlockSpec(memory_space=pltpu.HBM)
 BF16 = jnp.bfloat16
 F32 = jnp.float32
 NN, NT, TN = (((1,), (0,)), ((1,), (1,)), ((0,), (0,)))
@@ -178,17 +178,19 @@
 
 def layer_kernel(
     tok_hbm,
-    gain_ref,
+    gain_hbm,
     wq_hbm,
     wk_hbm,
     wv_hbm,
-    down_ref,
-    up_ref,
-    bias_ref,
-    shift_ref,
-    ogain_ref,
+    down_hbm,
+    up_hbm,
+    bias_hbm,
+    shift_hbm,
+    ogain_hbm,
     wo_hbm,
-    out_ref,
+    own_ref,
+    from_l,
+    from_r,
     tok_ref,
     xn,
     wkv,
@@ -212,8 +214,12 @@
     chip,
     ring_l,
     ring_r,
-    from_l,
-    from_r,
+    gain_ref,
+    down_ref,
+    up_ref,
+    bias_ref,
+    shift_ref,
+    ogain_ref,
     in_sem,
     tok_send,
     tok_recv,
@@ -247,6 +253,12 @@
         pltpu.make_async_copy(tok_hbm.at[pl.ds(64, 64)], tok_ref.at[pl.ds(64, 64)], in_sem.at[3]),
         pltpu.make_async_copy(wq_hbm, wqb.at[z, y], in_sem.at[4]),
         pltpu.make_async_copy(wo_hbm, wo.at[z, y], in_sem.at[5]),
+        pltpu.make_async_copy(gain_hbm, gain_ref, in_sem.at[6]),
+        pltpu.make_async_copy(down_hbm, down_ref, in_sem.at[7]),
+        pltpu.make_async_copy(up_hbm, up_ref, in_sem.at[8]),
+        pltpu.make_async_copy(bias_hbm, bias_ref, in_sem.at[9]),
+        pltpu.make_async_copy(shift_hbm, shift_ref, in_sem.at[10]),
+        pltpu.make_async_copy(ogain_hbm, ogain_ref, in_sem.at[11]),
     )
     for load in loads:
         load.start()
@@ -313,6 +325,7 @@
     pl.semaphore_wait(barrier, 17)
     start_push(kv)
     loads[2].wait()
+    loads[6].wait()
     norm(0)
     go(token(0, x, 0, right))
     go(to_mate(6, x, 0))
@@ -325,20 +338,24 @@
     relay(kv, 1)
     from_mate(6, x, 0)
     from_mate(7, x, 1)
+    for load in loads[7:]:
+        load.wait()
     gates(x)
+    relay(kv, 2)
     arrive(0, left, 0, 8)
     go(token(2, left, 0, right))
     arrive(3, right, 1, 9)
     go(token(5, right, 1, left))
-    relay(kv, 2)
     relay(kv, 3)
     arrive(1, left, 1, 10)
     arrive(4, right, 0, 11)
-    relay(kv, 4)
     loads[4].wait()
     start_push(qs)
+    relay(kv, 4)
     loads[5].wait()
     start_push(outs)
+    wait_push(qs)
+    relay(qs, 1)
     from_mate(8, left, 0)
     from_mate(10, left, 1)
     gates(left)
@@ -347,6 +364,7 @@
     gates(right)
     arrive(2, far_x, 0, 12)
     arrive(5, far_x, 1, 13)
+    relay(qs, 2)
     from_mate(12, far_x, 0)
     from_mate(13, far_x, 1)
     gates(far_x)
@@ -361,14 +379,15 @@
     state_ref[...] = jnp.zeros_like(state_ref)
 
     def absorb(i, carry):
-        @pl.when(i == 1)
+        @pl.when(i == 0)
         def _():
-            wait_push(qs)
-            relay(qs, 1)
-
-        @pl.when(i == 3)
+            relay(qs, 3)
+            wait_push(outs)
+            relay(outs, 1)
+
+        @pl.when(i == 2)
         def _():
-            relay(qs, 2)
+            relay(qs, 4)
 
         now = dot(xn[i].reshape(QUAD, D), wkv[...].reshape(D, DK + DV), NN).astype(BF16)
         kv_ref[pl.ds(pl.multiple_of(i * QUAD, QUAD), QUAD), :] = now
@@ -410,17 +429,10 @@
         most = ref.at[pl.ds(0, 63)]
         pltpu.make_async_copy(most, most, sem).wait()
 
+    relay(outs, 2)
     lax.fori_loop(1, 64, start_ask, 0)
     got[sp] = give[sp]
     decays[sp] = decay_out[...]
-    relay(qs, 3)
-    wait_push(outs)
-    relay(outs, 1)
-    relay(qs, 4)
-    relay(outs, 2)
-    for p in qs:
-        p.finish()
-    relay(outs, 3)
 
     def attend(i, carry):
         at = pl.ds(pl.multiple_of(i * QUAD, QUAD), QUAD)
@@ -448,6 +460,10 @@
         far_ref[at, :] = (reach * jnp.exp(base_ref[i])).astype(BF16)
         return carry
 
+    for p in qs:
+        p.finish()
+    lax.fori_loop(0, NX, attend, 0)
+    relay(outs, 3)
     wait_all(got, scan_recv.at[0])
     wait_all(decays, scan_recv.at[1])
 
@@ -458,10 +474,9 @@
     lax.fori_loop(0, 64, prefix, jnp.zeros((8, DK), F32))
     lax.fori_loop(1, 64, start_reply, 0)
     relay(outs, 4)
-    lax.fori_loop(0, NX, attend, 0)
-    carried[sp] = answer[sp]
     for p in outs:
         p.finish()
+    carried[sp] = answer[sp]
     wait_all(carried, scan_recv.at[2])
 
     halves = (pl.ds(0, 64), pl.ds(64, 64))
@@ -525,7 +540,7 @@
     swap(3).wait_recv()
     for i in (2, 3, 4, 5):
         hops[i].wait_recv()
-    out_ref[...] = (both(3, slice(None)) + from_l[...].astype(F32) + from_r[...].astype(F32)).astype(BF16)
+    own_ref[...] = both(3, slice(None))
 
     for s in sends:
         s.wait_send()
@@ -554,11 +569,27 @@
     out_gain,
     w_out,
 ):
-    return pl.pallas_call(
+    inputs = [
+        pltpu.with_memory_space_constraint(a, pltpu.HBM)
+        for a in (
+            tokens,
+            norm_gain[None],
+            w_query,
+            w_key,
+            w_value,
+            w_rank_down.T,
+            w_rank_up,
+            gate_bias[None],
+            decay_shift[None],
+            out_gain[None],
+            w_out.T,
+        )
+    ]
+    own, l, r = pl.pallas_call(
         layer_kernel,
-        out_shape=jax.ShapeDtypeStruct(tokens.shape, BF16),
-        in_specs=[ANY, VMEM, ANY, ANY, ANY, VMEM, VMEM, VMEM, VMEM, VMEM, ANY],
-        out_specs=VMEM,
+        out_shape=(jax.ShapeDtypeStruct(tokens.shape, F32),) + (jax.ShapeDtypeStruct(tokens.shape, BF16),) * 2,
+        in_specs=[HBM] * 11,
+        out_specs=(VMEM,) * 3,
         scratch_shapes=[
             pltpu.VMEM((128, D), BF16),
             pltpu.VMEM((NX, 2, 128, D), BF16),
@@ -583,9 +614,13 @@
             pltpu.VMEM((3, 128, D), BF16),
             pltpu.VMEM((64, D), BF16),
             pltpu.VMEM((64, D), BF16),
-            pltpu.VMEM((128, D), BF16),
-            pltpu.VMEM((128, D), BF16),
-            pltpu.SemaphoreType.DMA((6,)),
+            pltpu.VMEM((1, D), F32),
+            pltpu.VMEM((16, D), BF16),
+            pltpu.VMEM((16, DK), BF16),
+            pltpu.VMEM((1, DK), F32),
+            pltpu.VMEM((1, NX * QUAD), F32),
+            pltpu.VMEM((1, DV), F32),
+            pltpu.SemaphoreType.DMA((12,)),
             pltpu.SemaphoreType.DMA((14,)),
             pltpu.SemaphoreType.DMA((14,)),
             pltpu.SemaphoreType.DMA((2, 35)),
@@ -598,21 +633,10 @@
             pltpu.SemaphoreType.DMA((10,)),
         ],
         compiler_params=pltpu.CompilerParams(
-            collective_id=0, has_side_effects=True, vmem_limit_bytes=56 * 1024 * 1024
+            collective_id=0, has_side_effects=True, vmem_limit_bytes=40 * 1024 * 1024
         ),
-    )(
-        tokens,
-        norm_gain[None],
-        w_query,
-        w_key,
-        w_value,
-        w_rank_down.T,
-        w_rank_up,
-        gate_bias[None],
-        decay_shift[None],
-        out_gain[None],
-        w_out.T,
-    )
+    )(*inputs)
+    return (own + l.astype(F32) + r.astype(F32)).astype(BF16)
 
 
 def solution(mesh):

time: 108 us -> 103 us (0.954)
  Pallas kernels: 106 us -> 102 us
  local copies, waits for them, and re-layouts: 1.88 us -> 0 us
    pallas_call x1, Pallas kernels: 106 us -> 102 us  [on_device(): pl.pallas_call(layer_kernel, out_shape=(jax.ShapeDtypeStruct(tokens.shape...]
    unnamed x1 -> x0, local copies, waits for them, and re-layouts: 1.88 us -> none
where the time goes in v4:
time: 103 us
  Pallas kernels  102 us (99%)
    pallas_call x1, Pallas kernels, on_device(): pl.pallas_call(layer_kernel, out_shape=(jax.ShapeDtypeStruct(tokens.shape...  102 us

profile of v4, /device:TPU:1, one launch (start us, length us, event | category | flops | bytes accessed | tf_op | source)
XLA Modules:
  0.0 103.0 jit_solution(443892062328372402)
XLA Ops:
  0.0 102.0 %shard_map.109 = (f32[128,2048]{1,0:T(8,128)S(1)}, bf16[128,2048]{1,0:T(8,128)(2,1)S(1)}, bf16[128,2048]{1,0:T(8,128)(2,1)S(1)}) custom-call(bf16[128,2048]{1,0:T(8,128)(2,1)} %tok_hbm.1, f32[1,2048]{1,0:T(1,128)} %bitcast.8, bf16[32,256]{1,0:T(8,128)(2,1)} %wq_hbm.1, bf16[32,256]{1,0:T(8,128)(2,1)} %wk_hbm.1, bf16[32,512]{1,0:T(8,128)(2,1)} %wv_hbm.1, ...), custom_call_target="tpu_custom_call" | custom-call | tf_op jit(solution)/shard_map/pallas_call | solution.py:588
  102.1 1.0 add_convert_fusion

commit v5 on v4

--- a/solution.py
+++ b/solution.py
@@ -204,7 +204,6 @@
     far_ref,
     state_ref,
     give,
-    decay_out,
     got,
     decays,
     answer,
@@ -236,10 +235,6 @@
     sp = z * NY + y
     right, left, mate = lax.rem(x + 1, NX), lax.rem(x + NX - 1, NX), 1 - c
 
-    def peer(d):
-        p = lax.rem(sp + d, 64)
-        return {"z": lax.div(p, 8), "y": lax.rem(p, 8)}
-
     barrier = pltpu.get_barrier_semaphore()
     near = [{"x": right}, {"x": left}, {"c": mate}]
     near += [{a: lax.rem(i + d, 8)} for a, i in (("y", y), ("z", z)) for d in range(1, 8)]
@@ -314,11 +309,19 @@
         rank = dot(xn[i].reshape(QUAD, D), down_ref[...], NT).astype(BF16)
         pre = dot(rank, up_ref[...], NN) + bias_ref[...]
         logs = jnp.minimum(pre, 0.0) - jnp.log1p(jnp.exp(-jnp.abs(pre)))
-        ones = jnp.ones((8, DK), BF16)
-        shift = shift_ref[:, pl.ds(pl.multiple_of(i * QUAD, QUAD), QUAD)]
-        shifts = sum(dot(jnp.broadcast_to(t.astype(F32), (8, QUAD)).astype(BF16), ones, TN) for t in split3(shift)) * 0.125
-        hi, mid, low = split3(logs * (1.0 / TAU) + shifts)
-        cum_ref[i] = dot(lower, hi, NN) + (dot(lower, mid, NN) + dot(lower, low, NN))
+        hi, mid, low = split3(logs * (1.0 / TAU))
+        cum_ref[i] = cum_ref[i] + (dot(lower, hi, NN) + (dot(lower, mid, NN) + dot(lower, low, NN)))
+
+    def line_decay(d):
+        ref = decays.at[z, y]
+        return remote(ref, ref, scan_send.at[1], scan_recv.at[1], y=lax.rem(y + d, NY))
+
+    def plane_decay(d):
+        ref = decays.at[z]
+        return remote(ref, ref, scan_send.at[3], scan_recv.at[3], z=lax.rem(z + d, NZ))
+
+    def wait_decays(ref, sem):
+        pltpu.make_async_copy(ref, ref, sem).wait()
 
     loads[0].wait()
     loads[1].wait()
@@ -335,10 +338,15 @@
     go(to_mate(7, x, 1))
     go(token(1, x, 1, right))
     go(token(4, x, 0, left))
+    loads[10].wait()
+    for i in range(NX):
+        shift = jnp.broadcast_to(shift_ref[:, i * QUAD : (i + 1) * QUAD], (QUAD, QUAD))
+        hi, mid, low = split3(shift)
+        cum_ref[i] = dot(lower, hi, NT) + (dot(lower, mid, NT) + dot(lower, low, NT))
     relay(kv, 1)
     from_mate(6, x, 0)
     from_mate(7, x, 1)
-    for load in loads[7:]:
+    for load in loads[7:10] + loads[11:]:
         load.wait()
     gates(x)
     relay(kv, 2)
@@ -372,7 +380,9 @@
     for i in range(NX):
         base_ref[i] = base
         base = base + cum_ref[i, QUAD - 1 : QUAD]
-    decay_out[...] = jnp.exp(base)
+    decays[z, y] = jnp.exp(base)
+    for d in range(1, NY):
+        line_decay(d).start()
     for p in kv:
         p.finish()
 
@@ -388,6 +398,12 @@
         @pl.when(i == 2)
         def _():
             relay(qs, 4)
+
+        @pl.when(i == 2)
+        def _():
+            wait_decays(decays.at[0, pl.ds(0, NY - 1)], scan_recv.at[1])
+            for d in range(1, NZ):
+                plane_decay(d).start()
 
         now = dot(xn[i].reshape(QUAD, D), wkv[...].reshape(D, DK + DV), NN).astype(BF16)
         kv_ref[pl.ds(pl.multiple_of(i * QUAD, QUAD), QUAD), :] = now
@@ -403,36 +419,32 @@
 
     give[...] = state_ref[...].reshape(64, 8, DK).astype(BF16)
 
-    def ask(d):
-        p = peer(d)
-        j = p["z"] * NY + p["y"]
-        return (
-            remote(give.at[j], got.at[sp], scan_send.at[0], scan_recv.at[0], **p),
-            remote(decay_out, decays.at[sp], scan_send.at[1], scan_recv.at[1], **p),
-        )
-
-    def reply(d):
-        p = peer(d)
-        j = p["z"] * NY + p["y"]
-        return remote(answer.at[j], carried.at[sp], scan_send.at[2], scan_recv.at[2], **p)
-
-    def start_ask(d, carry):
-        for r in ask(d):
-            r.start()
-        return carry
-
-    def start_reply(d, carry):
-        reply(d).start()
-        return carry
+    columns = [lax.rem(y + d, NY) for d in range(NY)]
+
+    def ask(zz, yy):
+        remote(give.at[zz * NY + yy], got.at[sp], scan_send.at[0], scan_recv.at[0], z=zz, y=yy).start()
+
+    def reply(zz, yy):
+        remote(answer.at[zz * NY + yy], carried.at[sp], scan_send.at[2], scan_recv.at[2], z=zz, y=yy).start()
+
+    def to_all(send):
+        def line(d, carry):
+            zz = lax.rem(z + d, NZ)
+            for yy in columns:
+                send(zz, yy)
+            return carry
+
+        for yy in columns[1:]:
+            send(z, yy)
+        lax.fori_loop(1, NZ, line, 0)
 
     def wait_all(ref, sem):
         most = ref.at[pl.ds(0, 63)]
         pltpu.make_async_copy(most, most, sem).wait()
 
     relay(outs, 2)
-    lax.fori_loop(1, 64, start_ask, 0)
+    to_all(ask)
     got[sp] = give[sp]
-    decays[sp] = decay_out[...]
 
     def attend(i, carry):
         at = pl.ds(pl.multiple_of(i * QUAD, QUAD), QUAD)
@@ -462,17 +474,18 @@
 
     for p in qs:
         p.finish()
-    lax.fori_loop(0, NX, attend, 0)
+    lax.fori_loop(0, 2, attend, 0)
     relay(outs, 3)
+    lax.fori_loop(2, NX, attend, 0)
     wait_all(got, scan_recv.at[0])
-    wait_all(decays, scan_recv.at[1])
+    wait_decays(decays.at[pl.ds(0, NZ - 1)], scan_recv.at[3])
 
     def prefix(j, carry):
         answer[j] = carry.astype(BF16)
-        return decays[j] * carry + got[j].astype(F32)
+        return decays[lax.div(j, NY), lax.rem(j, NY)] * carry + got[j].astype(F32)
 
     lax.fori_loop(0, 64, prefix, jnp.zeros((8, DK), F32))
-    lax.fori_loop(1, 64, start_reply, 0)
+    to_all(reply)
     relay(outs, 4)
     for p in outs:
         p.finish()
@@ -548,7 +561,8 @@
         p.drain()
     sent = give.at[pl.ds(0, 63)]
     pltpu.make_async_copy(sent, sent, scan_send.at[0]).wait()
-    wait_all(decays, scan_send.at[1])
+    wait_decays(decays.at[0, pl.ds(0, NY - 1)], scan_send.at[1])
+    wait_decays(decays.at[pl.ds(0, NZ - 1)], scan_send.at[3])
     wait_all(answer, scan_send.at[2])
     for k in range(4):
         swap(k).wait_send()
@@ -604,9 +618,8 @@
             pltpu.VMEM((NX * QUAD, DK), BF16),
             pltpu.VMEM((DV, DK), F32),
             pltpu.VMEM((64, 8, DK), BF16),
-            pltpu.VMEM((1, DK), F32),
             pltpu.VMEM((64, 8, DK), BF16),
-            pltpu.VMEM((64, 1, DK), F32),
+            pltpu.VMEM((NZ, NY, 1, DK), F32),
             pltpu.VMEM((64, 8, DK), BF16),
             pltpu.VMEM((64, 8, DK), BF16),
             pltpu.VMEM((NX, 2, 128, D), BF16),
@@ -627,8 +640,8 @@
             pltpu.SemaphoreType.DMA((2, 35)),
             pltpu.SemaphoreType.DMA((4, 21)),
             pltpu.SemaphoreType.DMA((4, 21)),
-            pltpu.SemaphoreType.DMA((3,)),
-            pltpu.SemaphoreType.DMA((3,)),
+            pltpu.SemaphoreType.DMA((4,)),
+            pltpu.SemaphoreType.DMA((4,)),
             pltpu.SemaphoreType.DMA((10,)),
             pltpu.SemaphoreType.DMA((10,)),
         ],

time: 103 us -> 102 us (level)
    pallas_call x1, Pallas kernels: 102 us -> 101 us  [on_device(): pl.pallas_call(layer_kernel, out_shape=(jax.ShapeDtypeStruct(tokens.shape...]
where the time goes in v5:
time: 102 us
  Pallas kernels  101 us (99%)
    pallas_call x1, Pallas kernels, on_device(): pl.pallas_call(layer_kernel, out_shape=(jax.ShapeDtypeStruct(tokens.shape...  101 us

profile of v5, /device:TPU:1, one launch (start us, length us, event | category | flops | bytes accessed | tf_op | source)
XLA Modules:
  0.0 102.0 jit_solution(7935468251923112070)
XLA Ops:
  0.0 101.0 %shard_map.109 = (f32[128,2048]{1,0:T(8,128)S(1)}, bf16[128,2048]{1,0:T(8,128)(2,1)S(1)}, bf16[128,2048]{1,0:T(8,128)(2,1)S(1)}) custom-call(bf16[128,2048]{1,0:T(8,128)(2,1)} %tok_hbm.1, f32[1,2048]{1,0:T(1,128)} %bitcast.8, bf16[32,256]{1,0:T(8,128)(2,1)} %wq_hbm.1, bf16[32,256]{1,0:T(8,128)(2,1)} %wk_hbm.1, bf16[32,512]{1,0:T(8,128)(2,1)} %wv_hbm.1, ...), custom_call_target="tpu_custom_call" | custom-call | tf_op jit(solution)/shard_map/pallas_call | solution.py:602
  101.0 1.0 add_convert_fusion
